TPU v7x, 32 devices: a whole 2x2x4 slice. The times are simulated.
32 devices in a mesh: sp: 8 (over z, y), tp: 4 (over x, core).
Axes of the slice: x: 2, y: 2, z: 4, core: 2. Of those that a mesh axis runs over, the one named last changes fastest.
Arguments:
- tokens: bfloat16 [8192, 2048], P('sp', 'tp'), may hold values from -6 to 6
- mix_gain: float32 [2048], replicated, may hold values from 0.1 to 1.9
- query_weight: bfloat16 [2048, 1024], P('sp', 'tp'), may hold values from -0.125 to 0.125
- key_weight: bfloat16 [2048, 256], P('sp', 'tp'), may hold values from -0.125 to 0.125
- value_weight: bfloat16 [2048, 256], P('sp', 'tp'), may hold values from -0.125 to 0.125
- conv_value_weight: bfloat16 [2048, 1024], P('sp', 'tp'), may hold values from -0.125 to 0.125
- conv_gate_weight: bfloat16 [2048, 1024], P('sp', 'tp'), may hold values from -0.125 to 0.125
- query_gain: float32 [64], replicated, may hold values from 0.1 to 1.9
- key_gain: float32 [64], replicated, may hold values from 0.1 to 1.9
- sink_logit: float32 [16], P('tp'), may hold values from 3 to 7
- conv_taps: float32 [31, 1024], P(None, 'tp'), may hold values from -1 to 1
- conv_gain: float32 [1024], P('tp'), may hold values from 0.1 to 1.9
- attn_proj: bfloat16 [1024, 2048], P('tp', 'sp'), may hold values from -1.5 to 1.5
- conv_proj: bfloat16 [1024, 2048], P('tp', 'sp'), may hold values from -0.1875 to 0.1875
Outputs:
- mixed: bfloat16 [8192, 2048], P(('sp', 'tp'))
All inputs are finite; a program needn't handle non-finite values.
Results may differ from a plain program's by a relative error of at most 0.0079.
Values may be sent and summed in bfloat16 or wider, within the bound.
A program may use at most 128 MiB of HBM per device.

v0:
```python
import functools

import jax
import jax.numpy as jnp
from jax import lax
from jax.experimental import pallas as pl
from jax.experimental.pallas import tpu as pltpu
from jax.sharding import PartitionSpec as P

WINDOW = 128


EPSILON = 0.1


def padded(value, sides, width):
    for axis, dim in sides:
        size, length = (lax.axis_size(axis), value.shape[dim])
        up = [(i, (i + 1) % size) for i in range(size - 1)]
        down = [(j, i) for i, j in up]
        last = lax.slice_in_dim(value, length - width, length, axis=dim)
        leading = lax.slice_in_dim(value, 0, width, axis=dim)
        before = lax.ppermute(last, axis, up)
        after = lax.ppermute(leading, axis, down)
        value = jnp.concatenate([before, value, after], axis=dim)
    return value


def unit_rows(values, gain):
    return values * lax.rsqrt(jnp.mean(values * values, axis=-1, keepdims=True) + EPSILON) * gain


def attend(queries, keys, values, sinks, offset, total):
    count, local_kv, group, size = queries.shape
    scale = size ** (-0.5)
    blocks = count // WINDOW
    span = 3 * WINDOW

    def windows(rows):
        cut = rows.reshape(blocks + 2, WINDOW, local_kv, size)
        return jnp.concatenate([cut[:blocks], cut[1 : blocks + 1], cut[2:]], axis=1)

    cut_queries = queries.reshape(blocks, WINDOW, local_kv, group, size)
    scores = jnp.einsum(
        "bqkgd,bskd->bkgqs", cut_queries, windows(keys), preferred_element_type=jnp.float32
    )
    query_row = jnp.arange(WINDOW, dtype=jnp.int32)[None, :, None]
    key_row = jnp.arange(span, dtype=jnp.int32)[None, None, :] - WINDOW
    key_pos = offset + WINDOW * jnp.arange(blocks, dtype=jnp.int32)[:, None, None] + key_row
    allowed = (jnp.abs(key_row - query_row) <= WINDOW) & (key_pos >= 0) & (key_pos < total)
    weights = jnp.where(allowed[:, None, None], jnp.exp(scores * scale), 0.0)
    denominator = jnp.sum(weights, axis=-1) + jnp.exp(sinks).reshape(local_kv, group, 1)
    shares = (weights / denominator[..., None]).astype(jnp.bfloat16)
    result = jnp.einsum(
        "bkgqs,bskd->bqkgd", shares, windows(values), preferred_element_type=jnp.float32
    )
    return result.reshape(count, -1).astype(jnp.bfloat16)


def depthwise(extended, kernel_taps, count):
    result = jnp.zeros((count, kernel_taps.shape[1]), jnp.float32)
    for offset in range(kernel_taps.shape[0]):
        result = result + kernel_taps[offset] * extended[offset : offset + count]
    return result


def snake(size):
    if size % 2:
        return (lambda index: index), (lambda place: place)
    half = size // 2

    def place_of(index):
        odd = index % 2
        return (index // 2) * (1 - odd) + (size - 1 - index // 2) * odd

    def index_of(place):
        back = place // half
        return 2 * place * (1 - back) + (2 * (size - 1 - place) + 1) * back

    return place_of, index_of


def plain(size):
    return (lambda index: index), (lambda place: place)


def gather_kernel(rings, *refs):
    count = len(rings)
    shards, outs = refs[:count], refs[count : 2 * count]
    local_sem = refs[2 * count]
    sems = refs[2 * count + 1 :]
    barrier = pltpu.get_barrier_semaphore()
    plans = []
    for number, (axis, size, dim, order) in enumerate(rings):
        place_of, index_of = order(size)
        place = place_of(lax.axis_index(axis))
        at = lambda shift, p=place, f=index_of, n=size: f((p + shift + n) % n)
        plans.append((axis, size, dim, at, shards[number], outs[number], sems[2 * number : 2 * number + 2]))
        for shift in (1, -1):
            pl.semaphore_signal(
                barrier, inc=1, device_id={axis: at(shift)}, device_id_type=pl.DeviceIdType.MESH
            )

    def window(out, dim, shard, index, low, high):
        rows, columns = shard.shape
        if dim == 0:
            begin = pl.multiple_of(index * rows + low, 16)
            return out.at[pl.ds(begin, high - low), :]
        return out.at[pl.ds(low, high - low), pl.ds(pl.multiple_of(index * columns, 128), columns)]

    local = []
    for number, (axis, size, dim, at, shard, out, _) in enumerate(plans):
        copy = pltpu.make_async_copy(
            shard, window(out, dim, shard, at(0), 0, shard.shape[0]), local_sem.at[number]
        )
        copy.start()
        local.append(copy)
    pl.semaphore_wait(barrier, 2 * count)

    def hop(plan, step, way):
        axis, size, dim, at, shard, out, (send, recv) = plan
        rows = shard.shape[0]
        low, high = 0, rows
        if 2 * step == size:
            low, high = (0, rows // 2) if way == 1 else (rows // 2, rows)
        owner = at(-way * (step - 1))
        target = window(out, dim, shard, owner, low, high)
        source = shard.at[pl.ds(low, high - low), :] if step == 1 else target
        slot = 2 * (step - 1) + (way + 1) // 2
        return pltpu.make_async_remote_copy(
            src_ref=source,
            dst_ref=target,
            send_sem=send.at[slot],
            recv_sem=recv.at[slot],
            device_id={axis: at(way)},
            device_id_type=pl.DeviceIdType.MESH,
        )

    pending = {}
    steps = [(n, s) for n, plan in enumerate(plans) for s in range(1, plan[1] // 2 + 1)]
    steps.sort(key=lambda item: ((item[1] - 1) / (plans[item[0]][1] // 2), -plans[item[0]][1]))
    for number, step in steps:
        for way in (1, -1):
            if step > 1:
                pending[number, step - 1, way].wait_recv()
            copy = hop(plans[number], step, way)
            copy.start()
            pending[number, step, way] = copy
    for number, plan in enumerate(plans):
        for way in (1, -1):
            pending[number, plan[1] // 2, way].wait_recv()
    for copy in pending.values():
        copy.wait_send()
    for copy in local:
        copy.wait()


def gather_both(tokens, joined):
    tp, sp = lax.axis_size("tp"), lax.axis_size("sp")
    rings = (("tp", tp, 1, plain), ("sp", sp, 0, snake))
    sems = []
    for _, size, _, _ in rings:
        sems += [pltpu.SemaphoreType.DMA((2 * (size // 2),))] * 2
    return pl.pallas_call(
        functools.partial(gather_kernel, rings),
        out_shape=(
            jax.ShapeDtypeStruct((tokens.shape[0], tokens.shape[1] * tp), tokens.dtype),
            jax.ShapeDtypeStruct((joined.shape[0] * sp, joined.shape[1]), joined.dtype),
        ),
        in_specs=[pl.BlockSpec(memory_space=pltpu.VMEM)] * 2,
        out_specs=[pl.BlockSpec(memory_space=pl.ANY)] * 2,
        scratch_shapes=[pltpu.SemaphoreType.DMA((2,))] + sems,
        compiler_params=pltpu.CompilerParams(collective_id=0, has_side_effects=True),
    )(tokens, joined)


def on_device(
    tokens,
    mix_gain,
    query_weight,
    key_weight,
    value_weight,
    conv_value_weight,
    conv_gate_weight,
    query_gain,
    key_gain,
    sink_logit,
    conv_taps,
    conv_gain,
    attn_proj,
    conv_proj,
):
    count = tokens.shape[0]
    shards = (query_weight, conv_value_weight, conv_gate_weight, key_weight, value_weight)
    whole, joined = gather_both(tokens, jnp.concatenate(shards, axis=1))
    normed = unit_rows(whole.astype(jnp.float32), mix_gain).astype(jnp.bfloat16)
    product = jnp.dot(normed, joined, preferred_element_type=jnp.float32)
    cuts = []
    for shard in shards[:-1]:
        cuts.append((cuts[-1] if cuts else 0) + shard.shape[1])
    query, conv_value, conv_gate, key_part, value_part = jnp.split(product, cuts, axis=1)
    head_size = query_gain.shape[0]
    local_kv = key_part.shape[1] // head_size
    group = query.shape[1] // head_size // local_kv
    queries = unit_rows(query.reshape(count, local_kv, group, head_size), query_gain).astype(
        jnp.bfloat16
    )
    keys_normed = (
        unit_rows(key_part.reshape(count, local_kv, head_size), key_gain)
        .astype(jnp.bfloat16)
        .reshape(count, -1)
    )
    values_cast = value_part.astype(jnp.bfloat16)
    gated = (conv_value * jax.nn.sigmoid(conv_gate)).astype(jnp.bfloat16)
    reach = (conv_taps.shape[0] - 1) // 2
    kv_width = keys_normed.shape[1]
    paired = jnp.concatenate([keys_normed, values_cast], axis=1)
    extended = padded(paired, (("sp", 0),), WINDOW)
    key_rows = extended[:, :kv_width]
    value_rows = extended[:, kv_width:]
    conv_rows = padded(gated, (("sp", 0),), reach)
    offset = lax.axis_index("sp") * count
    total = count * lax.axis_size("sp")
    span_rows = key_rows.shape[0]
    attended = attend(
        queries,
        key_rows.reshape(span_rows, local_kv, head_size),
        value_rows.reshape(span_rows, local_kv, head_size),
        sink_logit,
        offset,
        total,
    )
    convolved = depthwise(conv_rows, conv_taps, count)
    channels, tp = conv_taps.shape[1], lax.axis_size("tp")
    local_mean = jnp.mean(convolved, axis=1)
    local_square = jnp.sum(jnp.square(convolved - local_mean[:, None]), axis=1)
    slot = (jnp.arange(tp) == lax.axis_index("tp")).astype(jnp.float32)[:, None, None]
    every = lax.psum(slot * jnp.stack([local_mean, local_square])[None], "tp")
    center = jnp.mean(every[:, 0], axis=0)
    spread = jnp.sum(every[:, 1] + channels * jnp.square(every[:, 0] - center), axis=0)
    spread = spread / (channels * tp)
    centered = convolved - center[:, None]
    featured = jax.nn.silu(centered * lax.rsqrt(spread[:, None] + EPSILON) * conv_gain).astype(
        jnp.bfloat16
    )
    stacked, _ = lax.optimization_barrier((jnp.concatenate([attn_proj, conv_proj], axis=0), joined))
    proj_full = lax.all_gather(stacked, "sp", axis=1, tiled=True)
    mixers = jnp.concatenate([attended, featured], axis=1)
    partial = jnp.dot(mixers, proj_full, preferred_element_type=jnp.float32).astype(jnp.bfloat16)
    return lax.psum_scatter(partial, "tp", scatter_dimension=0, tiled=True)


def solution(mesh):
    placed = (
        P("sp", "tp"),
        P(),
        P("sp", "tp"),
        P("sp", "tp"),
        P("sp", "tp"),
        P("sp", "tp"),
        P("sp", "tp"),
        P(),
        P(),
        P("tp"),
        P(None, "tp"),
        P("tp"),
        P("tp", "sp"),
        P("tp", "sp"),
    )
    return jax.shard_map(
        on_device, mesh=mesh, in_specs=placed, out_specs=P(("sp", "tp"), None), check_vma=False
    )
```

profile of v0, /device:TPU:0, one launch (start us, length us, event | category | flops | bytes accessed | tf_op | source)
XLA Modules:
  0.0 189.1 jit_solution(5664016875587076568)
XLA Ops:
  6.5 0.9 copy.42
  7.4 0.9 copy.43
  8.3 1.9 %concatenate.62.refs_1_ = bf16[256,896]{1,0:T(8,128)(2,1)} concatenate(bf16[256,256]{1,0:T(8,128)(2,1)} %param.16, bf16[256,256]{1,0:T(8,128)(2,1)} %param.19, bf16[256,256]{1,0:T(8,128)(2,1)} %param.20, bf16[256,64]{1,0:T(8,128)(2,1)S(1)} %copy.42, bf16[256,64]{1,0:T(8,128)(2,1)S(1)} %copy.43), dimensions={1} | concatenate | bytes 917504 | tf_op jit(solution)/shard_map/concatenate | solution.py:195
  10.2 48.8 %shard_map.136 = (bf16[1024,2048]{1,0:T(8,128)(2,1)}, bf16[2048,896]{1,0:T(8,128)(2,1)}) custom-call(bf16[1024,512]{1,0:T(8,128)(2,1)} %refs_0_.1, bf16[256,896]{1,0:T(8,128)(2,1)} %concatenate.62.refs_1_), custom_call_target="tpu_custom_call" | custom-call | tf_op jit(solution)/shard_map/pallas_call | solution.py:164
  59.0 3.2 %fusion = f32[1024]{0:T(1024)S(1)} fusion(bf16[1024,2048]{1,0:T(8,128)(2,1)} %get-tuple-element.8), kind=kLoop, calls=%fused_computation.2 | loop fusion | flops 6290432 | bytes 4198400 | tf_op jit(solution)/shard_map/reduce_sum | solution.py:30
  62.3 0.2 copy-done
  62.5 6.6 %fusion.4 = f32[1024,896]{1,0:T(8,128)S(1)} fusion(bf16[2048,896]{1,0:T(8,128)(2,1)} %get-tuple-element.9, bf16[1024,2048]{1,0:T(8,128)(2,1)S(1)} %copy-done, f32[2048]{0:T(1024)S(1)} %copy-done.8, f32[1024]{0:T(1024)S(1)} %add_rsqrt_fusion.2), kind=kOutput, calls=%fused_computation.8 | convolution fusion | flops 3766484992 | bytes 11546624 | tf_op jit(solution)/shard_map/dot_general | solution.py:197
  69.1 0.2 multiply_reduce_fusion.1
  69.3 0.1 split.44
  69.5 0.2 multiply_convert_fusion.2
  69.7 0.1 pad_maximum_fusion.5
  69.8 1.4 collective-permute-start
  71.2 1.3 collective-permute-start.1
  72.5 0.3 slice_multiply_fusion
  72.8 0.8 copy-done.3
  73.6 0.6 fusion.72
  74.2 4.5 %collective-permute-start.2 = (bf16[15,256]{1,0:T(8,128)(2,1)}, bf16[15,256]{1,0:T(8,128)(2,1)S(1)}, u32[]{:S(2)}, u32[]{:S(2)}) collective-permute-start(bf16[15,256]{1,0:T(8,128)(2,1)} %get-tuple-element.20), channel_id=1, source_target_pairs={{0,4},{4,8},{8,12},{12,16},{16,20},{20,24},{24,28},{1,5},{5,9},{9,... | collective-permute-start | bytes 23048 | tf_op jit(solution)/shard_map/ppermute | solution.py:23
  78.8 1.3 collective-permute-start.3
  80.1 0.7 pad_maximum_fusion.3
  80.8 0.2 reduce-scatter.2.cloned.1.call-start
  81.1 0.7 fusion.75
  81.7 0.6 fusion.76
  82.4 0.3 copy.50
  82.7 0.2 copy.61
  82.9 0.3 copy.51
  83.4 0.1 abs_compare_fusion
  83.6 0.8 multiply_convert_fusion.1
  84.4 1.2 and_and_fusion
  85.6 1.1 copy.48
  86.7 0.7 exp.22
  87.4 0.1 copy.45
  87.5 17.7 %fusion.71 = (f32[1024]{0:T(1024)S(1)}, f32[1024,256]{1,0:T(8,128)S(1)}) fusion(bf16[15,256]{1,0:T(8,128)(2,1)} %collective-permute-done.3, bf16[1024,256]{1,0:T(8,128)(2,1)} %copy-done.3, f32[256]{0:T(256)} %bitcast.151, f32[256]{0:T(256)} %bitcast.152, f32[256]{0:T(256)} %bitcast.123, f32[256]{0:T(256)} %bitcast.124, f32[256]{0:T(256)} %bitcast.125, ...), kind=kLoop, calls=%fused_computation.154 | loop fusion | flops 47971328 | bytes 1624064 | tf_op jit(solution)/shard_map/reduce_sum | solution.py:235
  105.3 0.4 multiply_reduce_fusion
  105.7 10.9 %psum.7 = f32[4,2,1024]{2,0,1:T(4,128)S(1)} all-reduce(f32[4,2,1024]{2,0,1:T(4,128)S(1)} %broadcast_multiply_fusion), channel_id=1, replica_groups=mesh['sp'=8,'tp'=4] {'tp'}, use_global_device_ids=true, to_apply=%region_6.7 | all-reduce | flops 8192 | bytes 65536 | tf_op jit(solution)/shard_map/psum | solution.py:238
  116.7 1.1 multiply_convert_fusion
  117.8 0.2 maximum_maximum_fusion
  118.0 0.2 fusion.73
  118.2 0.1 copy.47
  118.4 0.1 copy.49
  118.5 0.1 copy.44
  118.6 0.1 copy.46
  118.8 1.8 fusion.3
  120.7 1.6 fusion.13
  122.3 0.7 copy.59
  123.0 0.7 reshape.257
  123.6 9.8 %all-gather.2.cloned.1.call-done = bf16[512,2048]{1,0:T(8,128)(2,1)} async-done(((bf16[512,256]{1,0:T(8,128)(2,1)}), bf16[512,2048]{1,0:T(8,128)(2,1)}) %all-gather.2.cloned.1.call-update) | async-done | bytes 2097168 | tf_op jit(solution)/shard_map/all_gather | solution.py:247
  133.5 5.9 %convolution_convert_fusion = bf16[1024,2048]{1,0:T(8,128)(2,1)} fusion(bf16[512,2048]{1,0:T(8,128)(2,1)} %all-gather.2.cloned.1.call-done, bf16[1024,256]{1,0:T(8,128)(2,1)S(1)} %multiply_convert_fusion, bf16[1024,256]{1,0:T(8,128)(2,1)S(1)} %reshape.257), kind=kOutput, calls=%fused_computation.11 | convolution fusion | flops 2151677952 | bytes 7340032 | tf_op jit(solution)/shard_map/dot_general | solution.py:249
  139.4 42.9 %reduce-scatter.2.cloned.1.call-done = bf16[256,2048]{1,0:T(8,128)(2,1)} async-done(((bf16[1024,2048]{1,0:T(8,128)(2,1)}), bf16[256,2048]{1,0:T(8,128)(2,1)}) %reduce-scatter.2.cloned.1.call-update) | async-done | bytes 1048592 | tf_op jit(solution)/shard_map/reduce_scatter | solution.py:250
  (40 shorter events, 0.5 us)
Async XLA Ops:
  6.5 55.7 %copy-start.8 = (f32[2048]{0:T(1024)S(1)}, f32[2048]{0:T(1024)}, u32[]{:S(2)}) copy-start(f32[2048]{0:T(1024)} %param.15) | copy-start | bytes 24580
  6.5 126.9 %all-gather.2.cloned.1.call-start = ((), (), s32[]{:S(2)}) async-start(), calls=%async_computation.1 | async-start | bytes 2359296 | tf_op jit(solution)/shard_map/all_gather | solution.py:247
  59.0 3.5 %copy-start = (bf16[1024,2048]{1,0:T(8,128)(2,1)S(1)}, bf16[1024,2048]{1,0:T(8,128)(2,1)}, u32[]{:S(2)}) copy-start(bf16[1024,2048]{1,0:T(8,128)(2,1)} %get-tuple-element.8) | copy-start | bytes 12582916
  62.5 7.0 %copy-start.7 = (f32[64]{0:T(128)S(1)}, f32[64]{0:T(128)}, u32[]{:S(2)}) copy-start(f32[64]{0:T(128)} %param.22) | copy-start | bytes 772
  69.0 11.0 %copy-start.4 = (bf16[256,256]{1,0:T(8,128)(2,1)S(1)}, bf16[256,256]{1,0:T(8,128)(2,1)}, u32[]{:S(2)}) copy-start(bf16[256,256]{1,0:T(8,128)(2,1)} %param.27) | copy-start | bytes 393220
  69.1 11.0 %copy-start.5 = (bf16[256,256]{1,0:T(8,128)(2,1)S(1)}, bf16[256,256]{1,0:T(8,128)(2,1)}, u32[]{:S(2)}) copy-start(bf16[256,256]{1,0:T(8,128)(2,1)} %param.26) | copy-start | bytes 393220
  69.3 11.8 %copy-start.6 = (f32[31,256]{1,0:T(8,128)S(1)}, f32[31,256]{1,0:T(8,128)}, u32[]{:S(2)}) copy-start(f32[31,256]{1,0:T(8,128)} %param.24) | copy-start | bytes 95236
  69.7 1.5 copy-start.1
  69.8 48.0 %collective-permute-start = (bf16[128,128]{1,0:T(8,128)(2,1)S(1)}, bf16[128,128]{1,0:T(8,128)(2,1)S(1)}, u32[]{:S(2)}, u32[]{:S(2)}) collective-permute-start(bf16[128,128]{1,0:T(8,128)(2,1)S(1)} %get-tuple-element.18), channel_id=1, source_target_pairs={{0,4},{4,8},{8,12},{12,16},{16,20},{20,24},{24,28},{1,5},{5,9},{9,... | collective-permute-start | bytes 98312 | tf_op jit(solution)/shard_map/ppermute | solution.py:23
  71.2 46.5 %collective-permute-start.1 = (bf16[128,128]{1,0:T(8,128)(2,1)S(1)}, bf16[128,128]{1,0:T(8,128)(2,1)S(1)}, u32[]{:S(2)}, u32[]{:S(2)}) collective-permute-start(bf16[128,128]{1,0:T(8,128)(2,1)S(1)} %get-tuple-element.19), channel_id=1, source_target_pairs={{4,0},{8,4},{12,8},{16,12},{20,16},{24,20},{28,24},{5,1},{9,5},{13... | collective-permute-start | bytes 98312 | tf_op jit(solution)/shard_map/ppermute | solution.py:24
  72.8 0.8 copy-start.3
  74.2 13.3 %collective-permute-start.2 = (bf16[15,256]{1,0:T(8,128)(2,1)}, bf16[15,256]{1,0:T(8,128)(2,1)S(1)}, u32[]{:S(2)}, u32[]{:S(2)}) collective-permute-start(bf16[15,256]{1,0:T(8,128)(2,1)} %get-tuple-element.20), channel_id=1, source_target_pairs={{0,4},{4,8},{8,12},{12,16},{16,20},{20,24},{24,28},{1,5},{5,9},{9,... | collective-permute-start | bytes 23048 | tf_op jit(solution)/shard_map/ppermute | solution.py:23
  78.8 8.8 %collective-permute-start.3 = (bf16[15,256]{1,0:T(8,128)(2,1)}, bf16[15,256]{1,0:T(8,128)(2,1)}, u32[]{:S(2)}, u32[]{:S(2)}) collective-permute-start(bf16[15,256]{1,0:T(8,128)(2,1)} %get-tuple-element.21), channel_id=1, source_target_pairs={{4,0},{8,4},{12,8},{16,12},{20,16},{24,20},{28,24},{5,1},{9,5},{13... | collective-permute-start | bytes 23048 | tf_op jit(solution)/shard_map/ppermute | solution.py:24
  80.8 101.5 %reduce-scatter.2.cloned.1.call-start = ((), (), s32[]{:S(2)}) async-start(), calls=%async_computation.2 | async-start | bytes 5242880 | tf_op jit(solution)/shard_map/reduce_scatter | solution.py:250
  83.4 34.4 %copy-start.2 = (bf16[1024,64]{1,0:T(8,128)(2,1)S(1)}, bf16[1024,64]{1,0:T(8,128)(2,1)}, u32[]{:S(2)}) copy-start(bf16[1024,64]{1,0:T(8,128)(2,1)} %copy-done.1) | copy-start | bytes 393220
Sparse Core Ops, SparseCore 0:
  80.9 52.4 all-gather.1
  139.5 42.7 reduce-scatter.1
where the time goes:
time: 190 us; the launch traced here: 189 us
  waiting for transfers between devices  52.8 us (28%)
  Pallas kernels  48.8 us (26%)
  other arithmetic  26.6 us (14%)
  matrix products  15.9 us (8%)
  between operations  13.9 us (7%)
  local copies, waits for them, and re-layouts  11.6 us (6%)
  blocking collectives  10.9 us (6%)
  starting transfers between devices  8.77 us (5%)
    pallas_call x1, Pallas kernels, gather_both(): pl.pallas_call(functools.partial(gather_kernel, rings), out_shape=(jax.Sh...  48.8 us
    reduce_scatter x1, waiting for transfers between devices, on_device(): return lax.psum_scatter(partial, 'tp', scatter_dimension=0, tiled=True)  42.9 us
    reduce_sum x1, other arithmetic, on_device(): local_mean = jnp.mean(convolved, axis=1)  17.7 us
    psum x1, blocking collectives, on_device(): every = lax.psum(slot * jnp.stack([local_mean, local_square])[None], 'tp')  10.9 us
    all_gather x1, waiting for transfers between devices, on_device(): proj_full = lax.all_gather(stacked, 'sp', axis=1, tiled=True)  9.83 us
    dot_general x1, matrix products, on_device(): product = jnp.dot(normed, joined, preferred_element_type=jnp.float32)  6.58 us
    ppermute x2, starting transfers between devices, padded(): before = lax.ppermute(last, axis, up)  5.96 us
    dot_general x1, matrix products, on_device(): jnp.dot(mixers, proj_full, preferred_element_type=jnp.float32)  5.87 us
  transfers between devices with their start and end apart: 6, of which 2 were waited for; matrix products, arithmetic and copies ran while one was open for 17% of the time, Pallas kernels for 0%

commit v1 on v0

--- a/solution.py
+++ b/solution.py
@@ -174,6 +174,699 @@
     )(tokens, joined)
 
 
+LANES = 128
+MESH = pl.DeviceIdType.MESH
+
+
+def remote(source, target, sems, where):
+    return pltpu.make_async_remote_copy(
+        src_ref=source,
+        dst_ref=target,
+        send_sem=sems[0],
+        recv_sem=sems[1],
+        device_id=where,
+        device_id_type=MESH,
+    )
+
+
+def contract_last(left, right):
+    return lax.dot_general(
+        left, right, (((1,), (1,)), ((), ())), preferred_element_type=jnp.float32
+    )
+
+
+def matmul(left, right):
+    return jnp.dot(left, right, preferred_element_type=jnp.float32)
+
+
+def lane_index(shape):
+    return lax.broadcasted_iota(jnp.int32, shape, len(shape) - 1)
+
+
+def row_index(shape):
+    return lax.broadcasted_iota(jnp.int32, shape, len(shape) - 2)
+
+
+def aligned(value, multiple):
+    return value if isinstance(value, int) else pl.multiple_of(value, multiple)
+
+
+class Ring:
+    def __init__(self, size, groups, sems):
+        place_of, index_of = snake(size)
+        place = place_of(lax.axis_index("sp"))
+        self.at = lambda shift: index_of((place + shift + size) % size)
+        self.half = size // 2
+        self.groups = groups
+        self.sems = sems
+        self.copies = {}
+        self.done = []
+        self.queue = [
+            (group, step, piece, way)
+            for group, (pieces, _) in enumerate(groups)
+            for step in range(1, self.half + 1)
+            for piece in range(len(pieces))
+            for way in (1, -1)
+            if self.sent(group, step, piece, way)
+        ]
+
+    def sent(self, group, step, piece, way):
+        if step < self.half:
+            return True
+        return step == self.half and (piece in self.groups[group][1]) == (way == 1)
+
+    def send(self, group, step, piece, way):
+        ref = self.groups[group][0][piece](self.at(-way * (step - 1)))
+        copy = remote(ref, ref, next(self.sems), {"sp": self.at(way)})
+        copy.start()
+        self.copies[group, step, piece, way] = copy
+
+    def first(self, group):
+        for piece in range(len(self.groups[group][0])):
+            for way in (1, -1):
+                self.send(group, 1, piece, way)
+
+    def advance(self, number, arrived=None):
+        for _ in range(min(number, len(self.queue))):
+            group, step, piece, way = self.queue.pop(0)
+            self.copies[group, step, piece, way].wait_recv()
+            if step < self.half and self.sent(group, step + 1, piece, way):
+                self.send(group, step + 1, piece, way)
+            if arrived is not None:
+                arrived(group, step, piece, way)
+
+    def through(self, group, step, arrived=None):
+        number = sum(1 for item in self.queue if item[:2] <= (group, step))
+        self.advance(number, arrived)
+
+    def slot(self, step, way):
+        return 2 * self.half - 1 if step == self.half else 2 * step - (1 if way == 1 else 0)
+
+    def owner(self, slot):
+        step = (slot + 1) // 2
+        return self.at(-step if slot % 2 else step)
+
+
+def fused_kernel(
+    sp,
+    tokens,
+    query_w,
+    key_w,
+    value_w,
+    conv_value_w,
+    conv_gate_w,
+    attn_p,
+    conv_p,
+    gains,
+    sinks,
+    taps,
+    out,
+    whole,
+    normed,
+    query_all,
+    kv_all,
+    value_all,
+    gate_all,
+    attn_all,
+    conv_all,
+    attn_other,
+    conv_other,
+    spread_heads,
+    band,
+    eye,
+    gated,
+    edge_out,
+    edge_in,
+    convolved,
+    stat_out,
+    stat_in,
+    stat_rows,
+    queries,
+    key_low,
+    key_high,
+    value_low,
+    value_high,
+    halo_out,
+    halo_in,
+    mixers,
+    mixers_other,
+    part_out,
+    part_in,
+    near_sum,
+    local_sem,
+    send_sem,
+    recv_sem,
+):
+    count, features = tokens.shape
+    depth, width = query_w.shape
+    model = features * 4
+    columns = attn_p.shape[1]
+    block = count // 4
+    pad = gated.shape[1] - count
+    reach = (taps.shape[0] - 1) // 2
+    half_pad = pad // 2
+    head = LANES // 2
+    channels = taps.shape[1]
+    s, t = lax.axis_index("sp"), lax.axis_index("tp")
+    a, c = t // 2, t % 2
+    inner, outer = t + 1 - 2 * c, (t + 2) % 4
+    cross = outer + 1 - 2 * c
+    number = iter(range(10**6))
+
+    def sem_pairs():
+        while True:
+            i = next(number)
+            yield send_sem.at[i], recv_sem.at[i]
+
+    sems = sem_pairs()
+    sent = []
+
+    def push(source, target, where):
+        copy = remote(source, target, next(sems), where)
+        copy.start()
+        sent.append(copy)
+        return copy
+
+    def rows_of(owner, low, high):
+        return pl.ds(pl.multiple_of(owner * depth + low, 16), high - low)
+
+    def kv_columns(owner):
+        return pl.ds(pl.multiple_of(owner * depth, LANES), depth)
+
+    cut = depth * 3 // 4
+    ring = Ring(
+        sp,
+        (
+            (
+                (
+                    lambda o: value_all.at[rows_of(o, 0, depth), :],
+                    lambda o: gate_all.at[rows_of(o, 0, depth), :],
+                ),
+                (0,),
+            ),
+            (
+                (
+                    lambda o: query_all.at[rows_of(o, 0, cut), :],
+                    lambda o: query_all.at[rows_of(o, cut, depth), :],
+                    lambda o: kv_all.at[:, kv_columns(o)],
+                ),
+                (0,),
+            ),
+            ((lambda o: attn_all.at[o], lambda o: conv_all.at[o]), (0,)),
+        ),
+        sems,
+    )
+
+    local = []
+    for i, (source, target) in enumerate(
+        (
+            (tokens, whole.at[t]),
+            (conv_value_w, value_all.at[rows_of(s, 0, depth), :]),
+            (conv_gate_w, gate_all.at[rows_of(s, 0, depth), :]),
+            (query_w, query_all.at[rows_of(s, 0, depth), :]),
+            (key_w, kv_all.at[pl.ds(0, head), kv_columns(s)]),
+            (value_w, kv_all.at[pl.ds(head, head), kv_columns(s)]),
+            (attn_p, attn_all.at[s]),
+            (conv_p, conv_all.at[s]),
+        )
+    ):
+        copy = pltpu.make_async_copy(source, target, local_sem.at[i])
+        copy.start()
+        local.append(copy)
+
+    barrier = pltpu.get_barrier_semaphore()
+    following, preceding = (s + 1) % sp, (s + sp - 1) % sp
+    near_devices = [{"sp": ring.at(1)}, {"sp": ring.at(-1)}, {"sp": following}, {"sp": preceding}]
+    near_devices += [{"tp": inner}, {"tp": outer}, {"tp": cross}]
+    for where in near_devices:
+        pl.semaphore_signal(barrier, inc=1, device_id=where, device_id_type=MESH)
+    for copy in local:
+        copy.wait()
+    pl.semaphore_wait(barrier, len(near_devices))
+
+    ring.first(0)
+    mine = [whole.at[t, pl.ds(i * block, block), :] for i in range(4)]
+    over = [push(ref, ref, {"tp": outer}) for ref in mine]
+    beside = push(whole.at[t], whole.at[t], {"tp": inner})
+
+    square = (width, width)
+    spread_heads[...] = jnp.where(
+        row_index(square) // head == lane_index(square) // head, 1.0 / head, 0.0
+    ).astype(jnp.bfloat16)
+    tile = (LANES, LANES)
+    row, lane = row_index(tile), lane_index(tile)
+    band[0] = (lane >= row).astype(jnp.float32)
+    band[1] = (lane <= row).astype(jnp.float32)
+    eye[...] = (lane == row).astype(jnp.float32)
+    ones_low = jnp.where(lane < head, 1.0, 0.0)
+    for i in range(value_low.shape[0] // LANES):
+        rows = pl.ds(i * LANES, LANES)
+        low, high = ones_low, 1.0 - ones_low
+        if i == 0:
+            low, high = (jnp.where(s > 0, v, 0.0) for v in (low, high))
+        if i == value_low.shape[0] // LANES - 1:
+            low, high = (jnp.where(s < sp - 1, v, 0.0) for v in (low, high))
+        value_low[rows, LANES:] = low.astype(jnp.bfloat16)
+        value_high[rows, LANES:] = high.astype(jnp.bfloat16)
+
+    step_rows = 64
+
+    def norm_rows(i, carry):
+        rows = pl.ds(pl.multiple_of(i * step_rows, step_rows), step_rows)
+        total = jnp.zeros((step_rows, LANES), jnp.float32)
+        for j in range(4):
+            for k in range(features // LANES):
+                x = whole[j, rows, k * LANES : (k + 1) * LANES].astype(jnp.float32)
+                total = total + x * x
+        mean = jnp.sum(total, axis=1, keepdims=True) * (1.0 / model)
+        scale = jnp.broadcast_to(lax.rsqrt(mean + EPSILON), (step_rows, LANES))
+        for j in range(4):
+            for k in range(features // LANES):
+                x = whole[j, rows, k * LANES : (k + 1) * LANES].astype(jnp.float32)
+                at = j * features + k * LANES
+                gain = gains[:, at : at + LANES]
+                normed[rows, at : at + LANES] = (x * scale * gain).astype(jnp.bfloat16)
+        return carry
+
+    def norm_block(i):
+        over[i].wait_recv()
+        source = whole.at[outer, pl.ds(i * block, block), :]
+        forwards.append(push(source, source, {"tp": inner}))
+        if i == 0:
+            beside.wait_recv()
+        forwards[i].wait_recv()
+        per = block // step_rows
+        lax.fori_loop(i * per, (i + 1) * per, norm_rows, 0)
+
+    forwards = []
+    half = ring.half
+    ring.through(0, 1)
+    norm_block(0)
+    for step in range(2, half):
+        ring.through(0, step)
+        if step == half - 1:
+            ring.first(1)
+        if step == 2:
+            norm_block(1)
+        if step == 3:
+            norm_block(2)
+    for i in range(len(forwards), 4):
+        norm_block(i)
+    ring.through(0, half)
+    ring.through(1, 1)
+
+    def gate_block(i):
+        left = normed[i * block : (i + 1) * block, :]
+        value = matmul(left, value_all[...])
+        gate = matmul(left, gate_all[...])
+        result = (value * jax.nn.sigmoid(gate)).astype(jnp.bfloat16)
+        wide = result.astype(jnp.float32)
+        for j in range(channels // LANES):
+            gated[j, i * block + half_pad : (i + 1) * block + half_pad, :] = wide[
+                :, j * LANES : (j + 1) * LANES
+            ]
+        if i == 0:
+            edge_out[0] = result[:half_pad, :]
+        if i == 3:
+            edge_out[1] = result[block - half_pad :, :]
+
+    gate_block(0)
+    gate_block(3)
+    edges = [
+        push(edge_out.at[1], edge_in.at[0], {"sp": following}),
+        push(edge_out.at[0], edge_in.at[1], {"sp": preceding}),
+    ]
+    gate_block(1)
+    ring.advance(2)
+    gate_block(2)
+    ring.advance(2)
+
+    def conv_rows(i, carry):
+        start = i * LANES
+        parts = []
+        for j in range(channels // LANES):
+            lanes = slice(j * LANES, (j + 1) * LANES)
+            total = jnp.zeros((LANES, LANES), jnp.float32)
+            first = half_pad - reach
+            for shift in range(8):
+                offsets = [o for o in range(first, first + 2 * reach + 1) if o % 8 == shift]
+                high = offsets[-1] - shift
+                rows = gated[j, pl.ds(start + shift, LANES + high), :]
+                for o in offsets:
+                    tap = taps[o - first : o - first + 1, lanes]
+                    total = total + tap * rows[o - shift : o - shift + LANES]
+            convolved[pl.ds(pl.multiple_of(start, LANES), LANES), lanes] = total
+            parts.append(total)
+        mean = jnp.sum(sum(parts[1:], parts[0]), axis=1, keepdims=True) * (1.0 / channels)
+        squares = [jnp.square(part - mean) for part in parts]
+        square_sum = jnp.sum(sum(squares[1:], squares[0]), axis=1, keepdims=True)
+        stat_out[pl.ds(i, 1), :] = jnp.sum(mean * eye[...], axis=0, keepdims=True)
+        stat_out[pl.ds(i + count // LANES, 1), :] = jnp.sum(
+            square_sum * eye[...], axis=0, keepdims=True
+        )
+        return carry
+
+    blocks = count // LANES
+    quarter = blocks // 4
+    lax.fori_loop(quarter, 2 * quarter, conv_rows, 0)
+    ring.through(1, 2)
+    lax.fori_loop(2 * quarter, 3 * quarter, conv_rows, 0)
+    for side, edge in enumerate(edges):
+        edge.wait_recv()
+        inside = s > 0 if side == 0 else s < sp - 1
+        values = jnp.where(inside, edge_in[side].astype(jnp.float32), 0.0)
+        start = 0 if side == 0 else count + half_pad
+        for j in range(channels // LANES):
+            gated[j, start : start + half_pad, :] = values[:, j * LANES : (j + 1) * LANES]
+    lax.fori_loop(0, quarter, conv_rows, 0)
+    ring.advance(2)
+    lax.fori_loop(3 * quarter, blocks, conv_rows, 0)
+    stats = [
+        push(stat_out, stat_in.at[i], {"tp": peer}) for i, peer in enumerate((inner, outer, cross))
+    ]
+    ring.through(1, half - 1)
+    ring.first(2)
+    for stat in stats:
+        stat.wait_recv()
+    every = [stat_out[...]] + [stat_in[i] for i in range(3)]
+    means = [v[:blocks] for v in every]
+    center = (means[0] + means[1] + means[2] + means[3]) * 0.25
+    spread = sum(v[blocks:] for v in every) + channels * sum(jnp.square(m - center) for m in means)
+    stat_rows[:blocks] = center
+    stat_rows[blocks:] = lax.rsqrt(spread * (1.0 / (channels * 4)) + EPSILON)
+
+    def feature_rows(i, carry):
+        rows = pl.ds(pl.multiple_of(i * LANES, LANES), LANES)
+        middle = jnp.sum(stat_rows[pl.ds(i, 1), :] * eye[...], axis=1, keepdims=True)
+        scale = jnp.sum(stat_rows[pl.ds(i + blocks, 1), :] * eye[...], axis=1, keepdims=True)
+        for j in range(channels // LANES):
+            lanes = slice(j * LANES, (j + 1) * LANES)
+            gain = gains[:, model + j * LANES : model + (j + 1) * LANES]
+            value = (convolved[rows, lanes] - middle) * scale * gain
+            mixers[rows, width + j * LANES : width + (j + 1) * LANES] = (
+                value * jax.nn.sigmoid(value)
+            ).astype(jnp.bfloat16)
+        return carry
+
+    lax.fori_loop(0, blocks, feature_rows, 0)
+    far, near = (1 - a) * 2, a * 2
+    give = [
+        pl.ds(pl.multiple_of((base + 1 - c) * block, block), block) for base in (far, near)
+    ]
+    keep = [pl.ds(pl.multiple_of((base + c) * block, block), block) for base in (far, near)]
+    given_features = [
+        push(mixers.at[give[f], width:], mixers_other.at[f, :, width:], {"tp": inner})
+        for f in range(2)
+    ]
+    ring.through(1, half)
+
+    base = model + channels
+
+    def key_value_block(i):
+        keys, vals = kv_all[:head, :], kv_all[head:, :]
+        weights = jnp.concatenate([keys, vals, vals, keys], axis=0)
+        part = contract_last(normed[i * block : (i + 1) * block, :], weights)
+        scaled = part * head_scale(part) * gains[:, base + width : base + 2 * width]
+        lanes = lane_index(part.shape)
+        result = jnp.where((lanes < head) | (lanes >= 3 * head), scaled, part)
+        low, high = result[:, :LANES], result[:, LANES:]
+        is_low = lane_index(low.shape) < head
+        rows = slice(WINDOW + i * block, WINDOW + (i + 1) * block)
+        store_key_values(rows, low, high, is_low)
+        if i == 0:
+            halo_out[0] = low[:WINDOW].astype(jnp.bfloat16)
+        if i == 3:
+            halo_out[1] = low[block - WINDOW :].astype(jnp.bfloat16)
+
+    def head_scale(part):
+        squares = part * part
+        high = squares.astype(jnp.bfloat16)
+        low = (squares - high.astype(jnp.float32)).astype(jnp.bfloat16)
+        mean = matmul(high, spread_heads[...]) + matmul(low, spread_heads[...])
+        return lax.rsqrt(mean + EPSILON)
+
+    def store_key_values(rows, low, high, is_low):
+        key_low[rows, :] = jnp.where(is_low, low, 0.0).astype(jnp.bfloat16)
+        value_high[rows, :LANES] = jnp.where(is_low, 0.0, low).astype(jnp.bfloat16)
+        value_low[rows, :LANES] = jnp.where(is_low, high, 0.0).astype(jnp.bfloat16)
+        key_high[rows, :] = jnp.where(is_low, 0.0, high).astype(jnp.bfloat16)
+
+    def query_block(rows):
+        part = matmul(normed[rows, :], query_all[...])
+        queries[rows, :] = (part * head_scale(part) * gains[:, base : base + width]).astype(
+            jnp.bfloat16
+        )
+
+    def arrived(group, step, piece, way):
+        slot = ring.slot(step, way)
+        share(slot, piece)
+
+    shared = {}
+
+    def share(slot, piece):
+        owner = ring.owner(slot)
+        whole_ref, other_ref = ((attn_all, attn_other), (conv_all, conv_other))[piece]
+        shared[slot, piece] = push(whole_ref.at[owner], other_ref.at[owner], {"tp": inner})
+
+    key_value_block(0)
+    key_value_block(3)
+    halos = [
+        push(halo_out.at[1], halo_in.at[0], {"sp": following}),
+        push(halo_out.at[0], halo_in.at[1], {"sp": preceding}),
+    ]
+    share(0, 0)
+    share(0, 1)
+    key_value_block(1)
+    ring.advance(2, arrived)
+    key_value_block(2)
+    ring.advance(2, arrived)
+    query_block(give[0])
+    query_block(keep[0])
+    for side, halo in enumerate(halos):
+        halo.wait_recv()
+        inside = s > 0 if side == 0 else s < sp - 1
+        low = halo_in[side].astype(jnp.float32)
+        high = pltpu.roll(low, head, 1)
+        is_low = lane_index(low.shape) < head
+        start = 0 if side == 0 else WINDOW + count
+        rows = slice(start, start + WINDOW)
+        key_low[rows, :] = jnp.where(is_low, low, 0.0).astype(jnp.bfloat16)
+        key_high[rows, :] = jnp.where(is_low, 0.0, high).astype(jnp.bfloat16)
+        value_low[rows, :LANES] = jnp.where(is_low & inside, high, 0.0).astype(jnp.bfloat16)
+        value_high[rows, :LANES] = jnp.where(is_low | ~inside, 0.0, low).astype(jnp.bfloat16)
+
+    exponent = head ** (-0.5) * 1.4426950408889634
+    head_lanes = lane_index((1, LANES)) < head
+    sink_rows = [
+        jnp.exp(jnp.where(head_lanes, sinks[2 * i], sinks[2 * i + 1])) for i in range(2)
+    ]
+
+    def attend_rows(first):
+        def body(i, carry):
+            start = pl.multiple_of(first + i * WINDOW, WINDOW)
+            rows = pl.ds(start, WINDOW)
+            left = jnp.concatenate([queries[rows, :LANES], queries[rows, LANES:]], axis=0)
+            shares, vals = [], []
+            for j in range(3):
+                span = pl.ds(pl.multiple_of(start + j * WINDOW, WINDOW), WINDOW)
+                right = jnp.concatenate([key_low[span, :], key_high[span, :]], axis=0)
+                weight = jnp.exp2(contract_last(left, right) * exponent)
+                if j != 1:
+                    mask = band[j // 2]
+                    mask = jnp.concatenate([mask, mask], axis=0)
+                    weight = weight * jnp.concatenate([mask, mask], axis=1)
+                shares.append(weight.astype(jnp.bfloat16))
+                vals += [value_low[span, :], value_high[span, :]]
+            total = matmul(jnp.concatenate(shares, axis=1), jnp.concatenate(vals, axis=0))
+            for j in range(2):
+                piece = total[j * WINDOW : (j + 1) * WINDOW]
+                mixers[rows, j * LANES : (j + 1) * LANES] = (
+                    piece[:, :LANES] / (piece[:, LANES:] + sink_rows[j])
+                ).astype(jnp.bfloat16)
+            return carry
+
+        lax.fori_loop(0, block // WINDOW, body, 0)
+
+    def attend_half(f, base):
+        attend_rows((base + 1 - c) * block)
+        copy = push(mixers.at[give[f], :width], mixers_other.at[f, :, :width], {"tp": inner})
+        ring.advance(2, arrived)
+        attend_rows((base + c) * block)
+        return copy
+
+    given_heads = attend_half(0, far)
+    ring.advance(2, arrived)
+
+    def project(f, slot):
+        owner = ring.owner(slot)
+        left = jnp.concatenate([mixers[keep[f], :], mixers_other[f]], axis=1)
+        right = jnp.concatenate(
+            [attn_all[owner], conv_all[owner], attn_other[owner], conv_other[owner]], axis=0
+        )
+        return matmul(left, right)
+
+    parts = []
+
+    def send_part(slot):
+        for piece in range(2):
+            shared[slot, piece].wait_recv()
+        part_out[slot] = project(0, slot).astype(jnp.bfloat16)
+        parts.append(push(part_out.at[slot], part_in.at[slot], {"tp": outer}))
+
+    given_features[0].wait_recv()
+    given_heads.wait_recv()
+
+    def ready():
+        return [k for k in range(len(parts), sp) if all((k, p) in shared for p in range(2))]
+
+    def send_ready(most=sp):
+        for k in ready()[:most]:
+            if k == len(parts):
+                send_part(k)
+
+    send_ready()
+    query_block(give[1])
+    ring.advance(2, arrived)
+    query_block(keep[1])
+    ring.advance(2, arrived)
+    send_ready()
+    given_heads = attend_half(1, near)
+    ring.advance(2, arrived)
+    send_ready()
+    given_features[1].wait_recv()
+    given_heads.wait_recv()
+    for slot in range(len(parts)):
+        near_sum[slot] = project(1, slot)
+    done = len(parts)
+    while len(parts) < sp:
+        ring.advance(2, arrived)
+        send_ready()
+    for slot in range(done, sp):
+        near_sum[slot] = project(1, slot)
+    for slot in range(sp):
+        parts[slot].wait_recv()
+        owner = ring.owner(slot)
+        out[:, pl.ds(pl.multiple_of(owner * columns, LANES), columns)] = (
+            near_sum[slot] + part_in[slot].astype(jnp.float32)
+        ).astype(jnp.bfloat16)
+    for copy in sent:
+        copy.wait_send()
+    for copy in ring.copies.values():
+        copy.wait_send()
+
+
+def fits(sp, tp, tokens, query_weight, key_weight, conv_weight, attn_proj, taps, head):
+    return (
+        tp == 4
+        and sp % 2 == 0
+        and sp >= 6
+        and tokens.shape[0] % (4 * 2 * WINDOW) == 0
+        and tokens.shape[1] % LANES == 0
+        and WINDOW == LANES
+        and 2 * head == LANES
+        and key_weight.shape[1] == head
+        and query_weight.shape[1] == 4 * head
+        and conv_weight.shape[1] == 4 * head
+        and query_weight.shape[0] % LANES == 0
+        and attn_proj.shape[1] % LANES == 0
+        and taps.shape[0] <= 31
+    )
+
+
+def fused(
+    tokens,
+    mix_gain,
+    query_weight,
+    key_weight,
+    value_weight,
+    conv_value_weight,
+    conv_gate_weight,
+    query_gain,
+    key_gain,
+    sink_logit,
+    conv_taps,
+    conv_gain,
+    attn_proj,
+    conv_proj,
+):
+    sp = lax.axis_size("sp")
+    count, features = tokens.shape
+    model = features * 4
+    depth, width = query_weight.shape
+    head = query_gain.shape[0]
+    channels = conv_taps.shape[1]
+    columns = attn_proj.shape[1]
+    block = count // 4
+    plain_lanes = jnp.ones((2 * head,), jnp.float32)
+    gains = jnp.concatenate(
+        [mix_gain, conv_gain] + [query_gain] * 4 + [key_gain, plain_lanes, key_gain]
+    ).reshape(1, -1)
+    bf16, f32 = jnp.bfloat16, jnp.float32
+    copies = 160
+    half_pad = 16
+    scratch = [
+        pltpu.VMEM((4, count, features), bf16),
+        pltpu.VMEM((count, model), bf16),
+        pltpu.VMEM((model, width), bf16),
+        pltpu.VMEM((2 * head, model), bf16),
+        pltpu.VMEM((model, channels), bf16),
+        pltpu.VMEM((model, channels), bf16),
+        pltpu.VMEM((sp, width, columns), bf16),
+        pltpu.VMEM((sp, channels, columns), bf16),
+        pltpu.VMEM((sp, width, columns), bf16),
+        pltpu.VMEM((sp, channels, columns), bf16),
+        pltpu.VMEM((width, width), bf16),
+        pltpu.VMEM((2, LANES, LANES), f32),
+        pltpu.VMEM((LANES, LANES), f32),
+        pltpu.VMEM((channels // LANES, count + 2 * half_pad, LANES), f32),
+        pltpu.VMEM((2, half_pad, channels), bf16),
+        pltpu.VMEM((2, half_pad, channels), bf16),
+        pltpu.VMEM((count, channels), f32),
+        pltpu.VMEM((2 * count // LANES, LANES), f32),
+        pltpu.VMEM((3, 2 * count // LANES, LANES), f32),
+        pltpu.VMEM((2 * count // LANES, LANES), f32),
+        pltpu.VMEM((count, width), bf16),
+        pltpu.VMEM((count + 2 * WINDOW, LANES), bf16),
+        pltpu.VMEM((count + 2 * WINDOW, LANES), bf16),
+        pltpu.VMEM((count + 2 * WINDOW, 2 * LANES), bf16),
+        pltpu.VMEM((count + 2 * WINDOW, 2 * LANES), bf16),
+        pltpu.VMEM((2, WINDOW, LANES), bf16),
+        pltpu.VMEM((2, WINDOW, LANES), bf16),
+        pltpu.VMEM((count, width + channels), bf16),
+        pltpu.VMEM((2, block, width + channels), bf16),
+        pltpu.VMEM((sp, block, columns), bf16),
+        pltpu.VMEM((sp, block, columns), bf16),
+        pltpu.VMEM((sp, block, columns), f32),
+        pltpu.SemaphoreType.DMA((8,)),
+        pltpu.SemaphoreType.DMA((copies,)),
+        pltpu.SemaphoreType.DMA((copies,)),
+    ]
+    anywhere = pl.BlockSpec(memory_space=pl.ANY)
+    vmem = pl.BlockSpec(memory_space=pltpu.VMEM)
+    return pl.pallas_call(
+        functools.partial(fused_kernel, sp),
+        out_shape=jax.ShapeDtypeStruct((block, model), bf16),
+        in_specs=[anywhere] * 8 + [vmem, pl.BlockSpec(memory_space=pltpu.SMEM), vmem],
+        out_specs=vmem,
+        scratch_shapes=scratch,
+        compiler_params=pltpu.CompilerParams(
+            collective_id=1, has_side_effects=True, vmem_limit_bytes=56 * 2**20
+        ),
+    )(
+        tokens,
+        query_weight,
+        key_weight.T,
+        value_weight.T,
+        conv_value_weight,
+        conv_gate_weight,
+        attn_proj,
+        conv_proj,
+        gains,
+        sink_logit,
+        conv_taps,
+    )
+
+
 def on_device(
     tokens,
     mix_gain,
@@ -190,6 +883,33 @@
     attn_proj,
     conv_proj,
 ):
+    if fits(
+        lax.axis_size("sp"),
+        lax.axis_size("tp"),
+        tokens,
+        query_weight,
+        key_weight,
+        conv_value_weight,
+        attn_proj,
+        conv_taps,
+        query_gain.shape[0],
+    ):
+        return fused(
+            tokens,
+            mix_gain,
+            query_weight,
+            key_weight,
+            value_weight,
+            conv_value_weight,
+            conv_gate_weight,
+            query_gain,
+            key_gain,
+            sink_logit,
+            conv_taps,
+            conv_gain,
+            attn_proj,
+            conv_proj,
+        )
     count = tokens.shape[0]
     shards = (query_weight, conv_value_weight, conv_gate_weight, key_weight, value_weight)
     whole, joined = gather_both(tokens, jnp.concatenate(shards, axis=1))

time: 190 us -> 90.9 us (0.48)
  waiting for transfers between devices: 52.8 us -> 0 us
  Pallas kernels: 48.8 us -> 86.2 us
  other arithmetic: 26.6 us -> 0 us
  matrix products: 15.9 us -> 0 us
  between operations: 13.9 us -> 0.01 us
  blocking collectives: 10.9 us -> 0 us
  starting transfers between devices: 8.77 us -> 0 us
  local copies, waits for them, and re-layouts: 11.6 us -> 4.37 us
    reduce_scatter x1 -> x0, waiting for transfers between devices: 42.9 us -> none  [on_device(): return lax.psum_scatter(partial, 'tp', scatter_dimension=0, tiled=True)]
    pallas_call x1, Pallas kernels: 48.8 us -> 86.2 us  [fused(): pl.pallas_call(functools.partial(fused_kernel, sp), out_shape=jax.ShapeDt...]
    reduce_sum x7 -> x0, other arithmetic: 21.6 us -> none  [the longest x1 17.7 us: on_device(): local_mean = jnp.mean(convolved, axis=1)]
    dot_general x4 -> x0, matrix products: 15.9 us -> none  [the longest x1 6.58 us: on_device(): product = jnp.dot(normed, joined, preferred_element_type=jnp.float32)]
    psum x1 -> x0, blocking collectives: 10.9 us -> none  [on_device(): every = lax.psum(slot * jnp.stack([local_mean, local_square])[None], 'tp')]
    all_gather x1 -> x0, waiting for transfers between devices: 9.83 us -> none  [on_device(): proj_full = lax.all_gather(stacked, 'sp', axis=1, tiled=True)]
    ppermute x4 -> x0, starting transfers between devices: 8.55 us -> none  [the longest x2 5.96 us: padded(): before = lax.ppermute(last, axis, up)]
    slice x10 -> x0, local copies, waits for them, and re-layouts: 3.89 us -> none  [the longest x7 1.99 us: windows(): return jnp.concatenate([cut[:blocks], cut[1:blocks + 1], cut[2:]], axis=1)]
  transfers between devices with their start and end apart: 6 -> 0, of which waited for: 2 -> 0; matrix products, arithmetic and copies ran while one was open for 17% -> 0% of each run, Pallas kernels for 0% -> 0%
where the time goes in v1:
time: 90.9 us; the launch traced here: 90.6 us
  Pallas kernels  86.2 us (95%)
  local copies, waits for them, and re-layouts  4.37 us (5%)
    pallas_call x1, Pallas kernels, fused(): pl.pallas_call(functools.partial(fused_kernel, sp), out_shape=jax.ShapeDt...  86.2 us
    unnamed x7, local copies, waits for them, and re-layouts  2.99 us

profile of v1, /device:TPU:0, one launch (start us, length us, event | category | flops | bytes accessed | tf_op | source)
XLA Modules:
  0.0 90.6 jit_solution(586370969290076731)
XLA Ops:
  0.0 0.0 copy-start.2
  0.0 0.0 copy-start
  0.0 0.0 copy-start.1
  0.0 0.7 copy-done.2
  0.7 0.0 copy-done
  0.7 0.0 copy-done.1
  0.7 0.8 concatenate.3
  1.5 0.6 reshape.3.gains
  2.1 86.2 %shard_map.136 = bf16[256,2048]{1,0:T(8,128)(2,1)} custom-call(bf16[1024,512]{1,0:T(8,128)(2,1)} %tokens.1, bf16[256,256]{1,0:T(8,128)(2,1)} %query_w.1, bf16[64,256]{1,0:T(8,128)(2,1)} %bitcast.2, bf16[64,256]{1,0:T(8,128)(2,1)} %bitcast.3, bf16[256,256]{1,0:T(8,128)(2,1)} %conv_value_w.1, bf16[256,256]{1,0:T(8,128)(2,1)} %conv_gate_w.1, ...), custom_call_target="tpu_custom_call" | custom-call | tf_op jit(solution)/shard_map/pallas_call | solution.py:846
  88.3 2.3 %copy.16 = bf16[256,2048]{1,0:T(8,128)(2,1)} copy(bf16[256,2048]{1,0:T(8,128)(2,1)} %shard_map.136) | data formatting | bytes 2097152
  (1 shorter events, 0.0 us)
Async XLA Ops:
  0.0 0.7 copy-start.2
  0.0 0.7 copy-start
  0.0 0.7 copy-start.1

commit v2 on v0

--- a/solution.py
+++ b/solution.py
@@ -1,4 +1,5 @@
 import functools
+import types
 
 import jax
 import jax.numpy as jnp
@@ -174,6 +175,727 @@
     )(tokens, joined)
 
 
+LANES = 128
+MESH = pl.DeviceIdType.MESH
+
+
+def remote(source, target, sems, where):
+    return pltpu.make_async_remote_copy(
+        src_ref=source,
+        dst_ref=target,
+        send_sem=sems[0],
+        recv_sem=sems[1],
+        device_id=where,
+        device_id_type=MESH,
+    )
+
+
+def contract_last(left, right):
+    return lax.dot_general(
+        left, right, (((1,), (1,)), ((), ())), preferred_element_type=jnp.float32
+    )
+
+
+def matmul(left, right):
+    return jnp.dot(left, right, preferred_element_type=jnp.float32)
+
+
+def lane_index(shape):
+    return lax.broadcasted_iota(jnp.int32, shape, len(shape) - 1)
+
+
+def row_index(shape):
+    return lax.broadcasted_iota(jnp.int32, shape, len(shape) - 2)
+
+
+def aligned(value, multiple):
+    return value if isinstance(value, int) else pl.multiple_of(value, multiple)
+
+
+class Ring:
+    def __init__(self, size, groups, sems):
+        place_of, index_of = snake(size)
+        place = place_of(lax.axis_index("sp"))
+        self.at = lambda shift: index_of((place + shift + size) % size)
+        self.half = size // 2
+        self.groups = groups
+        self.sems = sems
+        self.copies = {}
+        self.arrived = None
+
+    def sent(self, group, step, piece, way):
+        if step < self.half:
+            return True
+        return step == self.half and (piece in self.groups[group][1]) == (way == 1)
+
+    def send(self, group, step, piece, way, source=None):
+        ref = self.groups[group][0][piece](self.at(-way * (step - 1)))
+        copy = remote(ref if source is None else source, ref, next(self.sems), {"sp": self.at(way)})
+        copy.start()
+        self.copies[group, step, piece, way] = copy
+
+    def first(self, group, sources=None):
+        for piece in range(len(self.groups[group][0])):
+            for way in (1, -1):
+                self.send(group, 1, piece, way, None if sources is None else sources[piece])
+
+    def take(self, group, step, piece=None):
+        for number in range(len(self.groups[group][0])):
+            for way in (1, -1):
+                if piece not in (None, number) or not self.sent(group, step, number, way):
+                    continue
+                with jax.named_scope(f"ring{group}_{step}_{number}"):
+                    self.copies[group, step, number, way].wait_recv()
+                if self.sent(group, step + 1, number, way):
+                    self.send(group, step + 1, number, way)
+                if self.arrived is not None:
+                    self.arrived(group, step, number, way)
+
+    def slot(self, step, way):
+        return 2 * self.half - 1 if step == self.half else 2 * step - (1 if way == 1 else 0)
+
+    def owner(self, slot):
+        step = (slot + 1) // 2
+        return self.at(-step if slot % 2 else step)
+
+
+def scoped(name):
+    def wrap(call):
+        def inner(*args):
+            with jax.named_scope(name):
+                return call(*args)
+
+        return inner
+
+    return wrap
+
+
+def fused_kernel(sp, names, *all_refs):
+    ref = types.SimpleNamespace(**dict(zip(names, all_refs)))
+    tokens, query_w, taps_w = ref.tokens, ref.query_w, ref.conv_taps
+    whole, normed, gated, convolved = ref.whole, ref.normed, ref.gated, ref.convolved
+    query_all, kv_all = ref.query_all, ref.kv_all
+    value_all, gate_all = ref.value_all, ref.gate_all
+    proj_all, proj_other = ref.proj_all, ref.proj_other
+    taps, sinks, mix_rows, conv_gains = ref.taps, ref.sinks, ref.mix_rows, ref.conv_gains
+    spread_heads, head_gains = ref.spread_heads, ref.head_gains
+    band, eye = ref.band, ref.eye
+    stat_out, stat_in, stat_rows = ref.stat_out, ref.stat_in, ref.stat_rows
+    queries = ref.queries
+    key_low, key_high = ref.key_low, ref.key_high
+    value_low, value_high = ref.value_low, ref.value_high
+    mixers, mixers_other = ref.mixers, ref.mixers_other
+    near_out, far_in, far_out = ref.near_out, ref.far_in, ref.far_out
+
+    count, features = tokens.shape
+    depth, width = query_w.shape
+    model = features * 4
+    columns = ref.attn_p.shape[1]
+    block = count // 4
+    half_pad = (gated.shape[1] - count) // 2
+    reach = (taps.shape[0] - 1) // 2
+    head = LANES // 2
+    channels = taps.shape[1]
+    blocks = count // LANES
+    s, t = lax.axis_index("sp"), lax.axis_index("tp")
+    a, c = t // 2, t % 2
+    inner, outer = t + 1 - 2 * c, (t + 2) % 4
+    cross = outer + 1 - 2 * c
+    send_sem, recv_sem, local_sem = ref.send_sem, ref.recv_sem, ref.local_sem
+
+    def sem_pairs():
+        for i in range(recv_sem.shape[0]):
+            yield send_sem, recv_sem.at[i]
+
+    sems = sem_pairs()
+    sent = []
+
+    def push(source, target, where):
+        copy = remote(source, target, next(sems), where)
+        copy.start()
+        sent.append(copy)
+        return copy
+
+    def rows_of(owner, low, high):
+        return pl.ds(pl.multiple_of(owner * depth + low, 16), high - low)
+
+    def kv_columns(owner):
+        return pl.ds(pl.multiple_of(owner * depth, LANES), depth)
+
+    def out_columns(owner):
+        return pl.ds(pl.multiple_of(owner * columns, LANES), columns)
+
+    cut = depth // 2
+    ring = Ring(
+        sp,
+        (
+            (
+                (
+                    lambda o: value_all.at[rows_of(o, 0, depth), :],
+                    lambda o: gate_all.at[rows_of(o, 0, depth), :],
+                ),
+                (0,),
+            ),
+            (
+                (
+                    lambda o: kv_all.at[pl.ds(0, head), kv_columns(o)],
+                    lambda o: kv_all.at[pl.ds(head, head), kv_columns(o)],
+                ),
+                (0,),
+            ),
+            (
+                (
+                    lambda o: query_all.at[rows_of(o, 0, cut), :],
+                    lambda o: query_all.at[rows_of(o, cut, depth), :],
+                ),
+                (0,),
+            ),
+            (
+                (
+                    lambda o: proj_all.at[o, pl.ds(0, width), :],
+                    lambda o: proj_all.at[o, pl.ds(width, channels), :],
+                ),
+                (0,),
+            ),
+        ),
+        sems,
+    )
+    half = ring.half
+
+    barrier = pltpu.get_barrier_semaphore()
+    following, preceding = (s + 1) % sp, (s + sp - 1) % sp
+    near_devices = [{"sp": ring.at(1)}, {"sp": ring.at(-1)}, {"sp": following}, {"sp": preceding}]
+    near_devices += [{"tp": inner}, {"tp": outer}, {"tp": cross}]
+    for where in near_devices:
+        pl.semaphore_signal(barrier, inc=1, device_id=where, device_id_type=MESH)
+    local = []
+    for i, (source, target) in enumerate(
+        (
+            (tokens, whole.at[t]),
+            (ref.key_w, kv_all.at[pl.ds(0, head), kv_columns(s)]),
+            (ref.value_w, kv_all.at[pl.ds(head, head), kv_columns(s)]),
+            (ref.mix_gain, mix_rows),
+            (query_w, query_all.at[rows_of(s, 0, depth), :]),
+            (ref.conv_value_w, value_all.at[rows_of(s, 0, depth), :]),
+            (ref.conv_gate_w, gate_all.at[rows_of(s, 0, depth), :]),
+            (ref.attn_p, proj_all.at[s, pl.ds(0, width), :]),
+            (ref.conv_p, proj_all.at[s, pl.ds(width, channels), :]),
+            (taps_w, taps),
+            (ref.sink_logit, sinks),
+            (ref.conv_gain, conv_gains),
+            (ref.query_gain, ref.query_gains),
+            (ref.key_gain, ref.key_gains),
+        )
+    ):
+        copy = pltpu.make_async_copy(source, target, local_sem.at[i])
+        copy.start()
+        local.append(copy)
+    with jax.named_scope("wait_barrier"):
+        pl.semaphore_wait(barrier, len(near_devices))
+
+    ring.first(0, (ref.conv_value_w, ref.conv_gate_w))
+    over = []
+    for i in range(4):
+        rows = pl.ds(i * block, block)
+        over.append(push(tokens.at[rows, :], whole.at[t, rows, :], {"tp": outer}))
+    beside = push(tokens, whole.at[t], {"tp": inner})
+    with jax.named_scope("wait_local"):
+        for copy in local:
+            copy.wait()
+
+    square = (width, width)
+    spread_heads[...] = jnp.where(
+        row_index(square) // head == lane_index(square) // head, 1.0 / head, 0.0
+    ).astype(jnp.bfloat16)
+    tile = (LANES, LANES)
+    row, lane = row_index(tile), lane_index(tile)
+    band[0] = (lane >= row).astype(jnp.float32)
+    band[1] = (lane <= row).astype(jnp.float32)
+    eye[...] = (lane == row).astype(jnp.float32)
+    query_gain, key_gain = ref.query_gains[...], ref.key_gains[...]
+    plain_lanes = jnp.ones_like(key_gain)
+    head_gains[0:1, :] = jnp.concatenate([query_gain] * 4, axis=1)
+    head_gains[1:2, :] = jnp.concatenate([key_gain, plain_lanes, plain_lanes, key_gain], axis=1)
+    ones_low = jnp.where(lane < head, 1.0, 0.0)
+    for i in range(value_low.shape[0] // LANES):
+        rows = pl.ds(i * LANES, LANES)
+        low, high = ones_low, 1.0 - ones_low
+        if i == 0:
+            low, high = (jnp.where(s > 0, v, 0.0) for v in (low, high))
+        if i == value_low.shape[0] // LANES - 1:
+            low, high = (jnp.where(s < sp - 1, v, 0.0) for v in (low, high))
+        value_low[rows, LANES:] = low.astype(jnp.bfloat16)
+        value_high[rows, LANES:] = high.astype(jnp.bfloat16)
+
+    step_rows = 64
+
+    def norm_rows(i, carry):
+        rows = pl.ds(pl.multiple_of(i * step_rows, step_rows), step_rows)
+        total = jnp.zeros((step_rows, LANES), jnp.float32)
+        for j in range(4):
+            for k in range(features // LANES):
+                x = whole[j, rows, k * LANES : (k + 1) * LANES].astype(jnp.float32)
+                total = total + x * x
+        mean = jnp.sum(total, axis=1, keepdims=True) * (1.0 / model)
+        scale = jnp.broadcast_to(lax.rsqrt(mean + EPSILON), (step_rows, LANES))
+        for j in range(4):
+            for k in range(features // LANES):
+                x = whole[j, rows, k * LANES : (k + 1) * LANES].astype(jnp.float32)
+                place = j * (features // LANES) + k
+                gain = mix_rows[place : place + 1, :]
+                normed[rows, place * LANES : (place + 1) * LANES] = (x * scale * gain).astype(
+                    jnp.bfloat16
+                )
+        return carry
+
+    forwards = []
+
+    def forward_tokens(i):
+        with jax.named_scope("wait_over"):
+            over[i].wait_recv()
+        source = whole.at[outer, pl.ds(i * block, block), :]
+        forwards.append(push(source, source, {"tp": inner}))
+
+    def norm_block(i):
+        with jax.named_scope("wait_forward"):
+            if i == 0:
+                beside.wait_recv()
+            forwards[i].wait_recv()
+        with jax.named_scope("norm"):
+            per = block // step_rows
+            lax.fori_loop(i * per, (i + 1) * per, norm_rows, 0)
+
+    edge_out, edge_in = ref.edge_out, ref.edge_in
+
+    @scoped("gate")
+    def gate_block(i):
+        left = normed[i * block : (i + 1) * block, :]
+        value = matmul(left, value_all[...])
+        gate = matmul(left, gate_all[...])
+        result = (value * jax.nn.sigmoid(gate)).astype(jnp.bfloat16)
+        wide = result.astype(jnp.float32)
+        for j in range(channels // LANES):
+            gated[j, i * block + half_pad : (i + 1) * block + half_pad, :] = wide[
+                :, j * LANES : (j + 1) * LANES
+            ]
+        if i == 0:
+            edge_out[0] = result[:half_pad, :]
+        if i == 3:
+            edge_out[1] = result[block - half_pad :, :]
+
+    def conv_rows(i, carry):
+        start = i * LANES
+        parts = []
+        for j in range(channels // LANES):
+            lanes = slice(j * LANES, (j + 1) * LANES)
+            total = jnp.zeros((LANES, LANES), jnp.float32)
+            first = half_pad - reach
+            for shift in range(8):
+                offsets = [o for o in range(first, first + 2 * reach + 1) if o % 8 == shift]
+                high = offsets[-1] - shift
+                rows = gated[j, pl.ds(start + shift, LANES + high), :]
+                for o in offsets:
+                    tap = taps[o - first : o - first + 1, lanes]
+                    total = total + tap * rows[o - shift : o - shift + LANES]
+            convolved[pl.ds(pl.multiple_of(start, LANES), LANES), lanes] = total
+            parts.append(total)
+        mean = jnp.sum(sum(parts[1:], parts[0]), axis=1, keepdims=True) * (1.0 / channels)
+        squares = [jnp.square(part - mean) for part in parts]
+        square_sum = jnp.sum(sum(squares[1:], squares[0]), axis=1, keepdims=True)
+        stat_out[pl.ds(i, 1), :] = jnp.sum(mean * eye[...], axis=0, keepdims=True)
+        stat_out[pl.ds(i + blocks, 1), :] = jnp.sum(square_sum * eye[...], axis=0, keepdims=True)
+        return carry
+
+    @scoped("conv")
+    def convolve(low, high):
+        lax.fori_loop(low, high, conv_rows, 0)
+
+    quarter = blocks // 4
+
+    def fill_edges():
+        for side, edge in enumerate(edges):
+            with jax.named_scope("wait_edge"):
+                edge.wait_recv()
+            inside = s > 0 if side == 0 else s < sp - 1
+            values = jnp.where(inside, edge_in[side].astype(jnp.float32), 0.0)
+            start = 0 if side == 0 else count + half_pad
+            for j in range(channels // LANES):
+                gated[j, start : start + half_pad, :] = values[:, j * LANES : (j + 1) * LANES]
+
+    def head_scale(part):
+        mean = matmul((part * part).astype(jnp.bfloat16), spread_heads[...])
+        return lax.rsqrt(mean + EPSILON)
+
+    halo_out, halo_in = ref.halo_out, ref.halo_in
+
+    @scoped("keys")
+    def key_value_block(i):
+        keys, vals = kv_all[:head, :], kv_all[head:, :]
+        weights = jnp.concatenate([keys, vals, vals, keys], axis=0)
+        part = contract_last(normed[i * block : (i + 1) * block, :], weights)
+        scaled = part * head_scale(part) * head_gains[1:2, :]
+        is_low = lane_index((block, LANES)) < head
+        rows = slice(WINDOW + i * block, WINDOW + (i + 1) * block)
+        key_low[rows, :] = jnp.where(is_low, scaled[:, :LANES], 0.0).astype(jnp.bfloat16)
+        value_high[rows, :LANES] = jnp.where(is_low, 0.0, part[:, :LANES]).astype(jnp.bfloat16)
+        value_low[rows, :LANES] = jnp.where(is_low, part[:, LANES:], 0.0).astype(jnp.bfloat16)
+        key_high[rows, :] = jnp.where(is_low, 0.0, scaled[:, LANES:]).astype(jnp.bfloat16)
+        if i in (0, 3):
+            low = jnp.where(is_low, scaled[:, :LANES], part[:, :LANES]).astype(jnp.bfloat16)
+            halo_out[i // 3] = low[:WINDOW] if i == 0 else low[block - WINDOW :]
+
+    ring.take(0, 1)
+    forward_tokens(0)
+    norm_block(0)
+    ring.take(0, 2)
+    ring.first(1)
+    forward_tokens(1)
+    norm_block(1)
+    for step in range(3, half):
+        ring.take(0, step)
+    ring.take(1, 1)
+    ring.first(2)
+    forward_tokens(2)
+    norm_block(2)
+    ring.take(0, half)
+    gate_block(0)
+    ring.take(1, 2)
+    forward_tokens(3)
+    gate_block(1)
+    ring.take(2, 1, 0)
+    norm_block(3)
+    ring.take(2, 1, 1)
+    gate_block(3)
+    edges = [
+        push(edge_out.at[1], edge_in.at[0], {"sp": following}),
+        push(edge_out.at[0], edge_in.at[1], {"sp": preceding}),
+    ]
+    for step in range(3, half):
+        ring.take(1, step)
+    gate_block(2)
+    ring.take(2, 2, 0)
+    convolve(quarter, 2 * quarter)
+    ring.take(2, 2, 1)
+    ring.take(1, half)
+    key_value_block(0)
+    key_value_block(3)
+    halos = [
+        push(halo_out.at[1], halo_in.at[0], {"sp": following}),
+        push(halo_out.at[0], halo_in.at[1], {"sp": preceding}),
+    ]
+    for step in range(3, half):
+        ring.take(2, step, 0)
+        convolve(2 * quarter, 3 * quarter) if step == 3 else None
+        ring.take(2, step, 1)
+    ring.first(3)
+    fill_edges()
+    convolve(0, quarter)
+    convolve(3 * quarter, blocks)
+    stats = [
+        push(stat_out, stat_in.at[i], {"tp": peer}) for i, peer in enumerate((inner, outer, cross))
+    ]
+    key_value_block(1)
+    key_value_block(2)
+    for stat in stats:
+        with jax.named_scope("wait_stat"):
+            stat.wait_recv()
+    every = [stat_out[...]] + [stat_in[i] for i in range(3)]
+    means = [v[:blocks] for v in every]
+    center = (means[0] + means[1] + means[2] + means[3]) * 0.25
+    spread = sum(v[blocks:] for v in every) + channels * sum(jnp.square(m - center) for m in means)
+    stat_rows[:blocks] = center
+    stat_rows[blocks:] = lax.rsqrt(spread * (1.0 / (channels * 4)) + EPSILON)
+
+    def feature_rows(i, carry):
+        rows = pl.ds(pl.multiple_of(i * LANES, LANES), LANES)
+        middle = jnp.sum(stat_rows[pl.ds(i, 1), :] * eye[...], axis=1, keepdims=True)
+        scale = jnp.sum(stat_rows[pl.ds(i + blocks, 1), :] * eye[...], axis=1, keepdims=True)
+        for j in range(channels // LANES):
+            lanes = slice(j * LANES, (j + 1) * LANES)
+            value = (convolved[rows, lanes] - middle) * scale * conv_gains[j : j + 1, :]
+            mixers[rows, width + j * LANES : width + (j + 1) * LANES] = (
+                value * jax.nn.sigmoid(value)
+            ).astype(jnp.bfloat16)
+        return carry
+
+    starts = ((1 - a) * 2, a * 2)
+    give = [pl.ds(pl.multiple_of((base + 1 - c) * block, block), block) for base in starts]
+    keep = [pl.ds(pl.multiple_of((base + c) * block, block), block) for base in starts]
+
+    @scoped("features")
+    def features_of(f):
+        low = starts[f] * (block // LANES)
+        lax.fori_loop(low, low + blocks // 2, feature_rows, 0)
+        return push(mixers.at[give[f], width:], mixers_other.at[f, :, width:], {"tp": inner})
+
+    given_features = [features_of(0)]
+    ring.take(2, half)
+
+    @scoped("queries")
+    def query_block(rows):
+        part = matmul(normed[rows, :], query_all[...])
+        queries[rows, :] = (part * head_scale(part) * head_gains[0:1, :]).astype(jnp.bfloat16)
+
+    shared = {}
+
+    def share(slot, piece):
+        owner = ring.owner(slot)
+        rows = pl.ds(piece * width, width if piece == 0 else channels)
+        pair = shared.get(slot) or next(sems)
+        shared[slot] = pair
+        copy = remote(
+            proj_all.at[owner, rows, :], proj_other.at[owner, rows, :], pair, {"tp": inner}
+        )
+        copy.start()
+        sent.append(copy)
+
+    ring.arrived = lambda group, step, piece, way: share(ring.slot(step, way), piece)
+    share(0, 0)
+    share(0, 1)
+    query_block(give[0])
+    query_block(keep[0])
+    ring.take(3, 1, 0)
+    for side, halo in enumerate(halos):
+        with jax.named_scope("wait_halo"):
+            halo.wait_recv()
+        inside = s > 0 if side == 0 else s < sp - 1
+        low = halo_in[side].astype(jnp.float32)
+        high = pltpu.roll(low, head, 1)
+        is_low = lane_index(low.shape) < head
+        start = 0 if side == 0 else WINDOW + count
+        rows = slice(start, start + WINDOW)
+        key_low[rows, :] = jnp.where(is_low, low, 0.0).astype(jnp.bfloat16)
+        key_high[rows, :] = jnp.where(is_low, 0.0, high).astype(jnp.bfloat16)
+        value_low[rows, :LANES] = jnp.where(is_low & inside, high, 0.0).astype(jnp.bfloat16)
+        value_high[rows, :LANES] = jnp.where(is_low | ~inside, 0.0, low).astype(jnp.bfloat16)
+
+    exponent = head ** (-0.5) * 1.4426950408889634
+    head_lanes = lane_index((1, LANES)) < head
+    sink_rows = [
+        jnp.exp(jnp.where(head_lanes, sinks[2 * i], sinks[2 * i + 1])) for i in range(2)
+    ]
+
+    @scoped("attend")
+    def attend_rows(first):
+        for i in range(block // WINDOW):
+            start = pl.multiple_of(first + i * WINDOW, WINDOW)
+            rows = pl.ds(start, WINDOW)
+            left = jnp.concatenate([queries[rows, :LANES], queries[rows, LANES:]], axis=0)
+            shares, vals = [], []
+            for j in range(3):
+                span = pl.ds(pl.multiple_of(start + j * WINDOW, WINDOW), WINDOW)
+                right = jnp.concatenate([key_low[span, :], key_high[span, :]], axis=0)
+                weight = jnp.exp2(contract_last(left, right) * exponent)
+                if j != 1:
+                    mask = band[j // 2]
+                    mask = jnp.concatenate([mask, mask], axis=0)
+                    weight = weight * jnp.concatenate([mask, mask], axis=1)
+                shares.append(weight.astype(jnp.bfloat16))
+                vals += [value_low[span, :], value_high[span, :]]
+            total = matmul(jnp.concatenate(shares, axis=1), jnp.concatenate(vals, axis=0))
+            for j in range(2):
+                piece = total[j * WINDOW : (j + 1) * WINDOW]
+                mixers[rows, j * LANES : (j + 1) * LANES] = (
+                    piece[:, :LANES] / (piece[:, LANES:] + sink_rows[j])
+                ).astype(jnp.bfloat16)
+
+    def attend_given(f):
+        attend_rows((starts[f] + 1 - c) * block)
+        return push(mixers.at[give[f], :width], mixers_other.at[f, :, :width], {"tp": inner})
+
+    def attend_kept(f):
+        attend_rows((starts[f] + c) * block)
+
+    @scoped("project")
+    def project(f, slot):
+        owner = ring.owner(slot)
+        left = jnp.concatenate([mixers[keep[f], :], mixers_other[f]], axis=1)
+        right = jnp.concatenate([proj_all[owner], proj_other[owner]], axis=0)
+        return matmul(left, right)
+
+    parts = []
+
+    def send_part(slot):
+        with jax.named_scope("wait_shared"):
+            block_ref = proj_other.at[ring.owner(slot)]
+            remote(block_ref, block_ref, shared[slot], {"tp": inner}).wait_recv()
+        far_out[slot] = project(0, slot).astype(jnp.bfloat16)
+        parts.append(
+            push(far_out.at[slot], far_in.at[:, out_columns(ring.owner(slot))], {"tp": outer})
+        )
+
+    def keep_part(slot):
+        near_out[:, out_columns(ring.owner(slot))] = project(1, slot)
+
+    given_heads = [attend_given(0)]
+    attend_kept(0)
+    with jax.named_scope("wait_given"):
+        given_features[0].wait_recv()
+        given_heads[0].wait_recv()
+    send_part(0)
+    ring.take(3, 1, 1)
+    given_features.append(features_of(1))
+    send_part(1)
+    send_part(2)
+    query_block(give[1])
+    ring.take(3, 2, 0)
+    query_block(keep[1])
+    given_heads.append(attend_given(1))
+    attend_kept(1)
+    with jax.named_scope("wait_given"):
+        given_features[1].wait_recv()
+        given_heads[1].wait_recv()
+    ring.take(3, 2, 1)
+    waiting = [0, 1, 2]
+    for step in range(2, half + 1):
+        keep_part(waiting.pop(0))
+        slots = (2 * step - 1, 2 * step) if step < half else (2 * step - 1,)
+        for slot in slots:
+            send_part(slot)
+            waiting.append(slot)
+        if step < half:
+            keep_part(waiting.pop(0))
+            ring.take(3, step + 1, 0)
+            if step + 1 < half:
+                keep_part(waiting.pop(0))
+            ring.take(3, step + 1, 1)
+    for slot in waiting:
+        keep_part(slot)
+    for slot in range(sp):
+        with jax.named_scope(f"wait_part{slot}"):
+            parts[slot].wait_recv()
+    with jax.named_scope("wait_sends"):
+        for copy in sent:
+            copy.wait_send()
+        for copy in ring.copies.values():
+            copy.wait_send()
+
+
+def recv_count(sp):
+    pieces = 4 * 2 * (2 * (sp // 2 - 1) + 1)
+    return pieces + 2 * sp + 9 + 2 + 2 + 3 + 4
+
+
+def fits(sp, tp, tokens, query_weight, key_weight, conv_weight, attn_proj, taps, head):
+    return (
+        tp == 4
+        and sp % 2 == 0
+        and sp >= 6
+        and tokens.shape[0] % (4 * 2 * WINDOW) == 0
+        and tokens.shape[1] % LANES == 0
+        and WINDOW == LANES
+        and 2 * head == LANES
+        and key_weight.shape[1] == head
+        and query_weight.shape[1] == 4 * head
+        and conv_weight.shape[1] == 4 * head
+        and query_weight.shape[0] % LANES == 0
+        and attn_proj.shape[1] % LANES == 0
+        and taps.shape[0] <= 31
+    )
+
+
+def fused(
+    tokens,
+    mix_gain,
+    query_weight,
+    key_weight,
+    value_weight,
+    conv_value_weight,
+    conv_gate_weight,
+    query_gain,
+    key_gain,
+    sink_logit,
+    conv_taps,
+    conv_gain,
+    attn_proj,
+    conv_proj,
+):
+    sp = lax.axis_size("sp")
+    count, features = tokens.shape
+    model = features * 4
+    depth, width = query_weight.shape
+    head = query_gain.shape[0]
+    channels = conv_taps.shape[1]
+    columns = attn_proj.shape[1]
+    block = count // 4
+    bf16, f32 = jnp.bfloat16, jnp.float32
+    half_pad = 16
+    stat = 2 * count // LANES
+    padded_rows = count + 2 * WINDOW
+    vmem, dma = pltpu.VMEM, pltpu.SemaphoreType.DMA
+    inputs = dict(
+        tokens=tokens,
+        query_w=query_weight,
+        key_w=key_weight.T,
+        value_w=value_weight.T,
+        conv_value_w=conv_value_weight,
+        conv_gate_w=conv_gate_weight,
+        attn_p=attn_proj,
+        conv_p=conv_proj,
+        mix_gain=mix_gain.reshape(-1, LANES),
+        conv_gain=conv_gain.reshape(-1, LANES),
+        query_gain=query_gain.reshape(1, -1),
+        key_gain=key_gain.reshape(1, -1),
+        sink_logit=sink_logit,
+        conv_taps=conv_taps,
+    )
+    outputs = dict(
+        near_out=vmem((block, model), f32),
+        far_in=vmem((block, model), bf16),
+    )
+    scratch = dict(
+        whole=vmem((4, count, features), bf16),
+        normed=vmem((count, model), bf16),
+        query_all=vmem((model, width), bf16),
+        kv_all=vmem((2 * head, model), bf16),
+        value_all=vmem((model, channels), bf16),
+        gate_all=vmem((model, channels), bf16),
+        proj_all=vmem((sp, width + channels, columns), bf16),
+        proj_other=vmem((sp, width + channels, columns), bf16),
+        taps=vmem(conv_taps.shape, f32),
+        sinks=pltpu.SMEM(sink_logit.shape, f32),
+        mix_rows=vmem((model // LANES, LANES), f32),
+        conv_gains=vmem((channels // LANES, LANES), f32),
+        query_gains=vmem((1, head), f32),
+        key_gains=vmem((1, head), f32),
+        head_gains=vmem((2, width), f32),
+        spread_heads=vmem((width, width), bf16),
+        band=vmem((2, LANES, LANES), f32),
+        eye=vmem((LANES, LANES), f32),
+        gated=vmem((channels // LANES, count + 2 * half_pad, LANES), f32),
+        edge_out=vmem((2, half_pad, channels), bf16),
+        edge_in=vmem((2, half_pad, channels), bf16),
+        convolved=vmem((count, channels), f32),
+        stat_out=vmem((stat, LANES), f32),
+        stat_in=vmem((3, stat, LANES), f32),
+        stat_rows=vmem((stat, LANES), f32),
+        queries=vmem((count, width), bf16),
+        key_low=vmem((padded_rows, LANES), bf16),
+        key_high=vmem((padded_rows, LANES), bf16),
+        value_low=vmem((padded_rows, 2 * LANES), bf16),
+        value_high=vmem((padded_rows, 2 * LANES), bf16),
+        halo_out=vmem((2, WINDOW, LANES), bf16),
+        halo_in=vmem((2, WINDOW, LANES), bf16),
+        mixers=vmem((count, width + channels), bf16),
+        mixers_other=vmem((2, block, width + channels), bf16),
+        far_out=vmem((sp, block, columns), bf16),
+        local_sem=dma((14,)),
+        send_sem=dma,
+        recv_sem=dma((recv_count(sp),)),
+    )
+    near, far = pl.pallas_call(
+        functools.partial(fused_kernel, sp, (*inputs, *outputs, *scratch)),
+        out_shape=tuple(outputs.values()),
+        in_specs=[pl.BlockSpec(memory_space=pltpu.HBM)] * len(inputs),
+        out_specs=[pl.BlockSpec(memory_space=pltpu.VMEM)] * 2,
+        scratch_shapes=list(scratch.values()),
+        compiler_params=pltpu.CompilerParams(
+            collective_id=1, has_side_effects=True, vmem_limit_bytes=60 * 2**20 + 2**19
+        ),
+    )(*inputs.values())
+    return (near + far.astype(f32)).astype(bf16)
+
+
 def on_device(
     tokens,
     mix_gain,
@@ -190,6 +912,33 @@
     attn_proj,
     conv_proj,
 ):
+    if fits(
+        lax.axis_size("sp"),
+        lax.axis_size("tp"),
+        tokens,
+        query_weight,
+        key_weight,
+        conv_value_weight,
+        attn_proj,
+        conv_taps,
+        query_gain.shape[0],
+    ):
+        return fused(
+            tokens,
+            mix_gain,
+            query_weight,
+            key_weight,
+            value_weight,
+            conv_value_weight,
+            conv_gate_weight,
+            query_gain,
+            key_gain,
+            sink_logit,
+            conv_taps,
+            conv_gain,
+            attn_proj,
+            conv_proj,
+        )
     count = tokens.shape[0]
     shards = (query_weight, conv_value_weight, conv_gate_weight, key_weight, value_weight)
     whole, joined = gather_both(tokens, jnp.concatenate(shards, axis=1))

time: 190 us -> 78.1 us (0.41)
  waiting for transfers between devices: 52.8 us -> 0 us
  Pallas kernels: 48.8 us -> 76.7 us
  other arithmetic: 26.6 us -> 1.26 us
  matrix products: 15.9 us -> 0 us
  between operations: 13.9 us -> 0.01 us
  local copies, waits for them, and re-layouts: 11.6 us -> 0 us
  blocking collectives: 10.9 us -> 0 us
  starting transfers between devices: 8.77 us -> 0 us
    reduce_scatter x1 -> x0, waiting for transfers between devices: 42.9 us -> none  [on_device(): return lax.psum_scatter(partial, 'tp', scatter_dimension=0, tiled=True)]
    pallas_call x1, Pallas kernels: 48.8 us -> 76.7 us  [fused(): pl.pallas_call(functools.partial(fused_kernel, sp, (*inputs, *outputs, *s...]
    reduce_sum x7 -> x0, other arithmetic: 21.6 us -> none  [the longest x1 17.7 us: on_device(): local_mean = jnp.mean(convolved, axis=1)]
    dot_general x4 -> x0, matrix products: 15.9 us -> none  [the longest x1 6.58 us: on_device(): product = jnp.dot(normed, joined, preferred_element_type=jnp.float32)]
    psum x1 -> x0, blocking collectives: 10.9 us -> none  [on_device(): every = lax.psum(slot * jnp.stack([local_mean, local_square])[None], 'tp')]
    all_gather x1 -> x0, waiting for transfers between devices: 9.83 us -> none  [on_device(): proj_full = lax.all_gather(stacked, 'sp', axis=1, tiled=True)]
    ppermute x4 -> x0, starting transfers between devices: 8.55 us -> none  [the longest x2 5.96 us: padded(): before = lax.ppermute(last, axis, up)]
    slice x10 -> x0, local copies, waits for them, and re-layouts: 3.89 us -> none  [the longest x7 1.99 us: windows(): return jnp.concatenate([cut[:blocks], cut[1:blocks + 1], cut[2:]], axis=1)]
  transfers between devices with their start and end apart: 6 -> 0, of which waited for: 2 -> 0; matrix products, arithmetic and copies ran while one was open for 17% -> 0% of each run, Pallas kernels for 0% -> 0%
where the time goes in v2:
time: 78.1 us; the launch traced here: 77.9 us
  Pallas kernels  76.7 us (98%)
  other arithmetic  1.26 us (2%)
    pallas_call x1, Pallas kernels, fused(): pl.pallas_call(functools.partial(fused_kernel, sp, (*inputs, *outputs, *s...  76.7 us

profile of v2, /device:TPU:0, one launch (start us, length us, event | category | flops | bytes accessed | tf_op | source)
XLA Modules:
  0.0 77.9 jit_solution(3100746947993753241)
XLA Ops:
  0.0 76.7 %shard_map.136 = (f32[256,2048]{1,0:T(8,128)S(1)}, bf16[256,2048]{1,0:T(8,128)(2,1)S(1)}) custom-call(bf16[1024,512]{1,0:T(8,128)(2,1)} %all_refs_0_.1, bf16[256,256]{1,0:T(8,128)(2,1)} %all_refs_1_.1, bf16[64,256]{1,0:T(8,128)(2,1)} %bitcast.6, bf16[64,256]{1,0:T(8,128)(2,1)} %bitcast.7, bf16[256,256]{1,0:T(8,128)(2,1)} %all_refs_4_.1, ...), custom_call_target="tpu_custom_call" | custom-call | tf_op jit(solution)/shard_map/pallas_call | solution.py:886
  76.7 1.3 %add_convert_fusion = bf16[256,2048]{1,0:T(8,128)(2,1)} fusion(f32[256,2048]{1,0:T(8,128)S(1)} %get-tuple-element.7, bf16[256,2048]{1,0:T(8,128)(2,1)S(1)} %get-tuple-element.8), kind=kLoop, calls=%fused_computation | loop fusion | flops 1572864 | bytes 4194304 | tf_op jit(solution)/shard_map/convert_element_type | solution.py:896

commit v3 on v2

--- a/solution.py
+++ b/solution.py
@@ -223,30 +223,31 @@
         self.copies = {}
         self.arrived = None
 
-    def sent(self, group, step, piece, way):
+    def part(self, group, step, piece, way):
+        whole, up, down = self.groups[group][piece]
         if step < self.half:
-            return True
-        return step == self.half and (piece in self.groups[group][1]) == (way == 1)
+            return whole
+        return None if step > self.half else up if way == 1 else down
 
     def send(self, group, step, piece, way, source=None):
-        ref = self.groups[group][0][piece](self.at(-way * (step - 1)))
+        ref = self.part(group, step, piece, way)(self.at(-way * (step - 1)))
         copy = remote(ref if source is None else source, ref, next(self.sems), {"sp": self.at(way)})
         copy.start()
         self.copies[group, step, piece, way] = copy
 
     def first(self, group, sources=None):
-        for piece in range(len(self.groups[group][0])):
+        for piece in range(len(self.groups[group])):
             for way in (1, -1):
                 self.send(group, 1, piece, way, None if sources is None else sources[piece])
 
     def take(self, group, step, piece=None):
-        for number in range(len(self.groups[group][0])):
+        for number in range(len(self.groups[group])):
             for way in (1, -1):
-                if piece not in (None, number) or not self.sent(group, step, number, way):
+                if piece not in (None, number) or self.part(group, step, number, way) is None:
                     continue
                 with jax.named_scope(f"ring{group}_{step}_{number}"):
                     self.copies[group, step, number, way].wait_recv()
-                if self.sent(group, step + 1, number, way):
+                if self.part(group, step + 1, number, way) is not None:
                     self.send(group, step + 1, number, way)
                 if self.arrived is not None:
                     self.arrived(group, step, number, way)
@@ -281,7 +282,7 @@
     spread_heads, head_gains = ref.spread_heads, ref.head_gains
     band, eye = ref.band, ref.eye
     stat_out, stat_in, stat_rows = ref.stat_out, ref.stat_in, ref.stat_rows
-    queries = ref.queries
+    queries, query_part = ref.queries, ref.query_part
     key_low, key_high = ref.key_low, ref.key_high
     value_low, value_high = ref.value_low, ref.value_high
     mixers, mixers_other = ref.mixers, ref.mixers_other
@@ -291,6 +292,7 @@
     depth, width = query_w.shape
     model = features * 4
     columns = ref.attn_p.shape[1]
+    thin = columns // 2
     block = count // 4
     half_pad = (gated.shape[1] - count) // 2
     reach = (taps.shape[0] - 1) // 2
@@ -310,8 +312,8 @@
     sems = sem_pairs()
     sent = []
 
-    def push(source, target, where):
-        copy = remote(source, target, next(sems), where)
+    def push(source, target, where, pair=None):
+        copy = remote(source, target, pair or next(sems), where)
         copy.start()
         sent.append(copy)
         return copy
@@ -326,37 +328,31 @@
         return pl.ds(pl.multiple_of(owner * columns, LANES), columns)
 
     cut = depth // 2
+
+    def value_piece(o):
+        return value_all.at[rows_of(o, 0, depth), :]
+
+    def gate_piece(o):
+        return gate_all.at[rows_of(o, 0, depth), :]
+
+    def kv_piece(low, high):
+        return lambda o: kv_all.at[pl.ds(low, high - low), kv_columns(o)]
+
+    def query_piece(low, high):
+        return lambda o: query_all.at[rows_of(o, low, high), :]
+
+    def proj_piece(piece):
+        return lambda o: proj_all.at[o, piece]
+
+    early, late = query_piece(0, cut), query_piece(cut, depth)
+    left_piece, right_piece = proj_piece(0), proj_piece(1)
     ring = Ring(
         sp,
         (
-            (
-                (
-                    lambda o: value_all.at[rows_of(o, 0, depth), :],
-                    lambda o: gate_all.at[rows_of(o, 0, depth), :],
-                ),
-                (0,),
-            ),
-            (
-                (
-                    lambda o: kv_all.at[pl.ds(0, head), kv_columns(o)],
-                    lambda o: kv_all.at[pl.ds(head, head), kv_columns(o)],
-                ),
-                (0,),
-            ),
-            (
-                (
-                    lambda o: query_all.at[rows_of(o, 0, cut), :],
-                    lambda o: query_all.at[rows_of(o, cut, depth), :],
-                ),
-                (0,),
-            ),
-            (
-                (
-                    lambda o: proj_all.at[o, pl.ds(0, width), :],
-                    lambda o: proj_all.at[o, pl.ds(width, channels), :],
-                ),
-                (0,),
-            ),
+            ((value_piece, value_piece, None), (gate_piece, None, gate_piece)),
+            ((kv_piece(0, 2 * head), kv_piece(0, head), kv_piece(head, 2 * head)),),
+            ((early, early, None), (late, None, late)),
+            ((left_piece, left_piece, None), (right_piece, None, right_piece)),
         ),
         sems,
     )
@@ -369,8 +365,7 @@
     for where in near_devices:
         pl.semaphore_signal(barrier, inc=1, device_id=where, device_id_type=MESH)
     local = []
-    for i, (source, target) in enumerate(
-        (
+    for source, target in (
             (tokens, whole.at[t]),
             (ref.key_w, kv_all.at[pl.ds(0, head), kv_columns(s)]),
             (ref.value_w, kv_all.at[pl.ds(head, head), kv_columns(s)]),
@@ -378,16 +373,17 @@
             (query_w, query_all.at[rows_of(s, 0, depth), :]),
             (ref.conv_value_w, value_all.at[rows_of(s, 0, depth), :]),
             (ref.conv_gate_w, gate_all.at[rows_of(s, 0, depth), :]),
-            (ref.attn_p, proj_all.at[s, pl.ds(0, width), :]),
-            (ref.conv_p, proj_all.at[s, pl.ds(width, channels), :]),
+            (ref.attn_p.at[:, :thin], proj_all.at[s, 0, pl.ds(0, width), :]),
+            (ref.attn_p.at[:, thin:], proj_all.at[s, 1, pl.ds(0, width), :]),
+            (ref.conv_p.at[:, :thin], proj_all.at[s, 0, pl.ds(width, channels), :]),
+            (ref.conv_p.at[:, thin:], proj_all.at[s, 1, pl.ds(width, channels), :]),
             (taps_w, taps),
             (ref.sink_logit, sinks),
             (ref.conv_gain, conv_gains),
             (ref.query_gain, ref.query_gains),
             (ref.key_gain, ref.key_gains),
-        )
     ):
-        copy = pltpu.make_async_copy(source, target, local_sem.at[i])
+        copy = pltpu.make_async_copy(source, target, local_sem)
         copy.start()
         local.append(copy)
     with jax.named_scope("wait_barrier"):
@@ -412,9 +408,10 @@
     band[0] = (lane >= row).astype(jnp.float32)
     band[1] = (lane <= row).astype(jnp.float32)
     eye[...] = (lane == row).astype(jnp.float32)
+    exponent = head ** (-0.5) * 1.4426950408889634
     query_gain, key_gain = ref.query_gains[...], ref.key_gains[...]
     plain_lanes = jnp.ones_like(key_gain)
-    head_gains[0:1, :] = jnp.concatenate([query_gain] * 4, axis=1)
+    head_gains[0:1, :] = jnp.concatenate([query_gain * exponent] * 4, axis=1)
     head_gains[1:2, :] = jnp.concatenate([key_gain, plain_lanes, plain_lanes, key_gain], axis=1)
     ones_low = jnp.where(lane < head, 1.0, 0.0)
     for i in range(value_low.shape[0] // LANES):
@@ -559,9 +556,10 @@
     norm_block(2)
     ring.take(0, half)
     gate_block(0)
+    gate_block(1)
     ring.take(1, 2)
     forward_tokens(3)
-    gate_block(1)
+    gate_block(2)
     ring.take(2, 1, 0)
     norm_block(3)
     ring.take(2, 1, 1)
@@ -570,41 +568,33 @@
         push(edge_out.at[1], edge_in.at[0], {"sp": following}),
         push(edge_out.at[0], edge_in.at[1], {"sp": preceding}),
     ]
+    convolve(quarter, quarter + 1)
     for step in range(3, half):
         ring.take(1, step)
-    gate_block(2)
+    convolve(quarter + 1, 3 * quarter - 1)
     ring.take(2, 2, 0)
-    convolve(quarter, 2 * quarter)
+    convolve(3 * quarter - 1, 3 * quarter)
+    convolve(1, quarter)
     ring.take(2, 2, 1)
+    convolve(3 * quarter, blocks - 1)
     ring.take(1, half)
+    fill_edges()
+    convolve(0, 1)
+    for step in range(3, half - 1):
+        ring.take(2, step)
+    convolve(blocks - 1, blocks)
+    stat_pair, part_pair = next(sems), next(sems)
+    for i, peer in enumerate((inner, outer, cross)):
+        push(stat_out, stat_in.at[i], {"tp": peer}, stat_pair)
+    ring.take(2, half - 1, 0)
     key_value_block(0)
+    right_halo = push(halo_out.at[0], halo_in.at[1], {"sp": preceding})
+    ring.take(2, half - 1, 1)
     key_value_block(3)
-    halos = [
-        push(halo_out.at[1], halo_in.at[0], {"sp": following}),
-        push(halo_out.at[0], halo_in.at[1], {"sp": preceding}),
-    ]
-    for step in range(3, half):
-        ring.take(2, step, 0)
-        convolve(2 * quarter, 3 * quarter) if step == 3 else None
-        ring.take(2, step, 1)
+    halos = [push(halo_out.at[1], halo_in.at[0], {"sp": following}), right_halo]
+    key_value_block(1)
     ring.first(3)
-    fill_edges()
-    convolve(0, quarter)
-    convolve(3 * quarter, blocks)
-    stats = [
-        push(stat_out, stat_in.at[i], {"tp": peer}) for i, peer in enumerate((inner, outer, cross))
-    ]
-    key_value_block(1)
     key_value_block(2)
-    for stat in stats:
-        with jax.named_scope("wait_stat"):
-            stat.wait_recv()
-    every = [stat_out[...]] + [stat_in[i] for i in range(3)]
-    means = [v[:blocks] for v in every]
-    center = (means[0] + means[1] + means[2] + means[3]) * 0.25
-    spread = sum(v[blocks:] for v in every) + channels * sum(jnp.square(m - center) for m in means)
-    stat_rows[:blocks] = center
-    stat_rows[blocks:] = lax.rsqrt(spread * (1.0 / (channels * 4)) + EPSILON)
 
     def feature_rows(i, carry):
         rows = pl.ds(pl.multiple_of(i * LANES, LANES), LANES)
@@ -628,56 +618,70 @@
         lax.fori_loop(low, low + blocks // 2, feature_rows, 0)
         return push(mixers.at[give[f], width:], mixers_other.at[f, :, width:], {"tp": inner})
 
+    @scoped("partial")
+    def partial_block(i, rows):
+        owners = [ring.owner(slot) for slot in range(sp - 1)]
+        left = jnp.concatenate([normed[rows, kv_columns(o)] for o in owners], axis=1)
+        right = jnp.concatenate([query_all[rows_of(o, 0, depth), :] for o in owners], axis=0)
+        query_part[i] = matmul(left, right)
+
+    @scoped("queries")
+    def query_block(i, rows):
+        owner = ring.owner(sp - 1)
+        last = matmul(normed[rows, kv_columns(owner)], query_all[rows_of(owner, 0, depth), :])
+        part = query_part[i] + last
+        queries[rows, :] = (part * head_scale(part) * head_gains[0:1, :]).astype(jnp.bfloat16)
+
+    far_rows = [give[0], keep[0]]
+    for i, rows in enumerate(far_rows):
+        partial_block(i, rows)
+    with jax.named_scope("wait_stat"):
+        remote(stat_in, stat_in, stat_pair, {"tp": inner}).wait_recv()
+    every = [stat_out[...]] + [stat_in[i] for i in range(3)]
+    means = [v[:blocks] for v in every]
+    center = (means[0] + means[1] + means[2] + means[3]) * 0.25
+    spread = sum(v[blocks:] for v in every) + channels * sum(jnp.square(m - center) for m in means)
+    stat_rows[:blocks] = center
+    stat_rows[blocks:] = lax.rsqrt(spread * (1.0 / (channels * 4)) + EPSILON)
+
     given_features = [features_of(0)]
     ring.take(2, half)
-
-    @scoped("queries")
-    def query_block(rows):
-        part = matmul(normed[rows, :], query_all[...])
-        queries[rows, :] = (part * head_scale(part) * head_gains[0:1, :]).astype(jnp.bfloat16)
+    for i, rows in enumerate(far_rows):
+        query_block(i, rows)
 
     shared = {}
 
     def share(slot, piece):
         owner = ring.owner(slot)
-        rows = pl.ds(piece * width, width if piece == 0 else channels)
-        pair = shared.get(slot) or next(sems)
-        shared[slot] = pair
-        copy = remote(
-            proj_all.at[owner, rows, :], proj_other.at[owner, rows, :], pair, {"tp": inner}
-        )
-        copy.start()
-        sent.append(copy)
+        source, target = proj_all.at[owner, piece], proj_other.at[owner, piece]
+        shared[slot, piece] = push(source, target, {"tp": inner})
 
     ring.arrived = lambda group, step, piece, way: share(ring.slot(step, way), piece)
     share(0, 0)
     share(0, 1)
-    query_block(give[0])
-    query_block(keep[0])
-    ring.take(3, 1, 0)
-    for side, halo in enumerate(halos):
-        with jax.named_scope("wait_halo"):
-            halo.wait_recv()
-        inside = s > 0 if side == 0 else s < sp - 1
-        low = halo_in[side].astype(jnp.float32)
-        high = pltpu.roll(low, head, 1)
-        is_low = lane_index(low.shape) < head
-        start = 0 if side == 0 else WINDOW + count
-        rows = slice(start, start + WINDOW)
-        key_low[rows, :] = jnp.where(is_low, low, 0.0).astype(jnp.bfloat16)
-        key_high[rows, :] = jnp.where(is_low, 0.0, high).astype(jnp.bfloat16)
-        value_low[rows, :LANES] = jnp.where(is_low & inside, high, 0.0).astype(jnp.bfloat16)
-        value_high[rows, :LANES] = jnp.where(is_low | ~inside, 0.0, low).astype(jnp.bfloat16)
-
-    exponent = head ** (-0.5) * 1.4426950408889634
+    def fill_halos():
+        for side, halo in enumerate(halos):
+            with jax.named_scope("wait_halo"):
+                halo.wait_recv()
+            inside = s > 0 if side == 0 else s < sp - 1
+            low = halo_in[side].astype(jnp.float32)
+            high = pltpu.roll(low, head, 1)
+            is_low = lane_index(low.shape) < head
+            start = 0 if side == 0 else WINDOW + count
+            rows = slice(start, start + WINDOW)
+            key_low[rows, :] = jnp.where(is_low, low, 0.0).astype(jnp.bfloat16)
+            key_high[rows, :] = jnp.where(is_low, 0.0, high).astype(jnp.bfloat16)
+            value_low[rows, :LANES] = jnp.where(is_low & inside, high, 0.0).astype(jnp.bfloat16)
+            value_high[rows, :LANES] = jnp.where(is_low | ~inside, 0.0, low).astype(jnp.bfloat16)
+
     head_lanes = lane_index((1, LANES)) < head
     sink_rows = [
         jnp.exp(jnp.where(head_lanes, sinks[2 * i], sinks[2 * i + 1])) for i in range(2)
     ]
 
     @scoped("attend")
-    def attend_rows(first):
-        for i in range(block // WINDOW):
+    def attend_rows(first, windows):
+        for i in range(windows):
             start = pl.multiple_of(first + i * WINDOW, WINDOW)
             rows = pl.ds(start, WINDOW)
             left = jnp.concatenate([queries[rows, :LANES], queries[rows, LANES:]], axis=0)
@@ -685,7 +689,7 @@
             for j in range(3):
                 span = pl.ds(pl.multiple_of(start + j * WINDOW, WINDOW), WINDOW)
                 right = jnp.concatenate([key_low[span, :], key_high[span, :]], axis=0)
-                weight = jnp.exp2(contract_last(left, right) * exponent)
+                weight = jnp.exp2(contract_last(left, right))
                 if j != 1:
                     mask = band[j // 2]
                     mask = jnp.concatenate([mask, mask], axis=0)
@@ -699,71 +703,110 @@
                     piece[:, :LANES] / (piece[:, LANES:] + sink_rows[j])
                 ).astype(jnp.bfloat16)
 
-    def attend_given(f):
-        attend_rows((starts[f] + 1 - c) * block)
-        return push(mixers.at[give[f], :width], mixers_other.at[f, :, :width], {"tp": inner})
-
-    def attend_kept(f):
-        attend_rows((starts[f] + c) * block)
+    def attend_given(f, low=0, size=block):
+        here = pl.multiple_of((starts[f] + 1 - c) * block + low, WINDOW)
+        attend_rows(here, size // WINDOW)
+        target = mixers_other.at[f, pl.ds(aligned(low, WINDOW), size), :width]
+        return push(mixers.at[pl.ds(here, size), :width], target, {"tp": inner})
+
+    def attend_kept(f, low=0, size=block):
+        attend_rows((starts[f] + c) * block + low, size // WINDOW)
 
     @scoped("project")
-    def project(f, slot):
+    def project(f, slot, pieces=(0, 1), low=0, size=block):
         owner = ring.owner(slot)
-        left = jnp.concatenate([mixers[keep[f], :], mixers_other[f]], axis=1)
-        right = jnp.concatenate([proj_all[owner], proj_other[owner]], axis=0)
-        return matmul(left, right)
-
-    parts = []
-
-    def send_part(slot):
+        here = pl.ds(pl.multiple_of((starts[f] + c) * block + low, WINDOW), size)
+        left = jnp.concatenate(
+            [mixers[here, :], mixers_other[f, pl.ds(aligned(low, WINDOW), size), :]], axis=1
+        )
+        right = [
+            jnp.concatenate([proj_all[owner, piece], proj_other[owner, piece]], axis=0)
+            for piece in pieces
+        ]
+        return matmul(left, jnp.concatenate(right, axis=1))
+
+    def wait_shared(slot, piece):
         with jax.named_scope("wait_shared"):
-            block_ref = proj_other.at[ring.owner(slot)]
-            remote(block_ref, block_ref, shared[slot], {"tp": inner}).wait_recv()
-        far_out[slot] = project(0, slot).astype(jnp.bfloat16)
-        parts.append(
-            push(far_out.at[slot], far_in.at[:, out_columns(ring.owner(slot))], {"tp": outer})
-        )
+            shared[slot, piece].wait_recv()
+
+    def send_rows(slot, low, size):
+        rows = pl.ds(aligned(low, WINDOW), size)
+        result = project(0, slot, (0, 1), low, size).astype(jnp.bfloat16)
+        for piece in range(2):
+            far_out[slot, piece, rows, :] = result[:, piece * thin : (piece + 1) * thin]
+        for piece in range(2):
+            target = far_in.at[rows, half_columns(slot, piece)]
+            push(far_out.at[slot, piece, rows, :], target, {"tp": outer}, part_pair)
+
+    def send_piece(slot, piece):
+        wait_shared(slot, piece)
+        far_out[slot, piece] = project(0, slot, (piece,)).astype(jnp.bfloat16)
+        target = far_in.at[:, half_columns(slot, piece)]
+        push(far_out.at[slot, piece], target, {"tp": outer}, part_pair)
+
+    def half_columns(slot, piece):
+        begin = ring.owner(slot) * columns + piece * thin
+        return pl.ds(pl.multiple_of(begin, LANES), thin)
 
     def keep_part(slot):
         near_out[:, out_columns(ring.owner(slot))] = project(1, slot)
 
-    given_heads = [attend_given(0)]
-    attend_kept(0)
+    split = block // 2
+    order = (a * split, (1 - a) * split)
+    given_heads = [attend_given(0, order[0], split)]
+    attend_kept(0, order[0], split)
+    given_features[0].wait_recv()
+    for piece in range(2):
+        wait_shared(0, piece)
     with jax.named_scope("wait_given"):
-        given_features[0].wait_recv()
         given_heads[0].wait_recv()
-    send_part(0)
-    ring.take(3, 1, 1)
-    given_features.append(features_of(1))
-    send_part(1)
-    send_part(2)
-    query_block(give[1])
-    ring.take(3, 2, 0)
-    query_block(keep[1])
-    given_heads.append(attend_given(1))
-    attend_kept(1)
+    send_rows(0, order[0], split)
+    fill_halos()
+    given_heads.append(attend_given(0, order[1], split))
+    attend_kept(0, order[1], split)
     with jax.named_scope("wait_given"):
-        given_features[1].wait_recv()
         given_heads[1].wait_recv()
-    ring.take(3, 2, 1)
-    waiting = [0, 1, 2]
-    for step in range(2, half + 1):
-        keep_part(waiting.pop(0))
+    send_rows(0, order[1], split)
+
+    def near_heads():
+        given_heads.append(attend_given(1))
+
+    def near_kept():
+        attend_kept(1)
+        with jax.named_scope("wait_given"):
+            given_features[1].wait_recv()
+            given_heads[2].wait_recv()
+
+    work = [
+        lambda: partial_block(0, give[1]),
+        lambda: query_block(0, give[1]),
+        lambda: given_features.append(features_of(1)),
+        lambda: partial_block(1, keep[1]),
+        lambda: query_block(1, keep[1]),
+        near_heads,
+        near_kept,
+        lambda: keep_part(0),
+    ]
+
+    def do_work(most):
+        for _ in range(min(most, len(work))):
+            work.pop(0)()
+
+    counts = {(1, 0): (1, 0), (1, 1): (1, 3), (2, 0): (1, 1), (2, 1): (1, 2)}
+    for step in range(1, half + 1):
         slots = (2 * step - 1, 2 * step) if step < half else (2 * step - 1,)
-        for slot in slots:
-            send_part(slot)
-            waiting.append(slot)
-        if step < half:
-            keep_part(waiting.pop(0))
-            ring.take(3, step + 1, 0)
-            if step + 1 < half:
-                keep_part(waiting.pop(0))
-            ring.take(3, step + 1, 1)
-    for slot in waiting:
-        keep_part(slot)
-    for slot in range(sp):
-        with jax.named_scope(f"wait_part{slot}"):
-            parts[slot].wait_recv()
+        for piece in range(2):
+            ring.take(3, step, piece)
+            before, after = counts.get((step, piece), (1, 1))
+            do_work(before)
+            for slot in slots:
+                send_piece(slot, piece)
+            if piece == 1:
+                work += [functools.partial(keep_part, slot) for slot in slots]
+            do_work(after)
+    do_work(len(work))
+    with jax.named_scope("wait_part"):
+        remote(far_in, far_in, part_pair, {"tp": outer}).wait_recv()
     with jax.named_scope("wait_sends"):
         for copy in sent:
             copy.wait_send()
@@ -772,8 +815,8 @@
 
 
 def recv_count(sp):
-    pieces = 4 * 2 * (2 * (sp // 2 - 1) + 1)
-    return pieces + 2 * sp + 9 + 2 + 2 + 3 + 4
+    pieces = 7 * 2 * (sp // 2 - 1) + 4 * 2
+    return pieces + 2 * sp + 9 + 2 + 2 + 2 + 2 + 3
 
 
 def fits(sp, tp, tokens, query_weight, key_weight, conv_weight, attn_proj, taps, head):
@@ -789,7 +832,7 @@
         and query_weight.shape[1] == 4 * head
         and conv_weight.shape[1] == 4 * head
         and query_weight.shape[0] % LANES == 0
-        and attn_proj.shape[1] % LANES == 0
+        and attn_proj.shape[1] % (2 * LANES) == 0
         and taps.shape[0] <= 31
     )
 
@@ -850,8 +893,8 @@
         kv_all=vmem((2 * head, model), bf16),
         value_all=vmem((model, channels), bf16),
         gate_all=vmem((model, channels), bf16),
-        proj_all=vmem((sp, width + channels, columns), bf16),
-        proj_other=vmem((sp, width + channels, columns), bf16),
+        proj_all=vmem((sp, 2, width + channels, columns // 2), bf16),
+        proj_other=vmem((sp, 2, width + channels, columns // 2), bf16),
         taps=vmem(conv_taps.shape, f32),
         sinks=pltpu.SMEM(sink_logit.shape, f32),
         mix_rows=vmem((model // LANES, LANES), f32),
@@ -870,6 +913,7 @@
         stat_in=vmem((3, stat, LANES), f32),
         stat_rows=vmem((stat, LANES), f32),
         queries=vmem((count, width), bf16),
+        query_part=vmem((2, block, width), f32),
         key_low=vmem((padded_rows, LANES), bf16),
         key_high=vmem((padded_rows, LANES), bf16),
         value_low=vmem((padded_rows, 2 * LANES), bf16),
@@ -878,8 +922,8 @@
         halo_in=vmem((2, WINDOW, LANES), bf16),
         mixers=vmem((count, width + channels), bf16),
         mixers_other=vmem((2, block, width + channels), bf16),
-        far_out=vmem((sp, block, columns), bf16),
-        local_sem=dma((14,)),
+        far_out=vmem((sp, 2, block, columns // 2), bf16),
+        local_sem=dma,
         send_sem=dma,
         recv_sem=dma((recv_count(sp),)),
     )

time: 78.1 us -> 75.1 us (0.962)
  Pallas kernels: 76.7 us -> 73.7 us
    pallas_call x1, Pallas kernels: 76.7 us -> 73.7 us  [fused(): pl.pallas_call(functools.partial(fused_kernel, sp, (*inputs, *outputs, *s...]
where the time goes in v3:
time: 75.1 us; the launch traced here: 75 us
  Pallas kernels  73.7 us (98%)
  other arithmetic  1.26 us (2%)
    pallas_call x1, Pallas kernels, fused(): pl.pallas_call(functools.partial(fused_kernel, sp, (*inputs, *outputs, *s...  73.7 us

profile of v3, /device:TPU:0, one launch (start us, length us, event | category | flops | bytes accessed | tf_op | source)
XLA Modules:
  0.0 75.0 jit_solution(7586817313270371912)
XLA Ops:
  0.0 73.7 %shard_map.136 = (f32[256,2048]{1,0:T(8,128)S(1)}, bf16[256,2048]{1,0:T(8,128)(2,1)S(1)}) custom-call(bf16[1024,512]{1,0:T(8,128)(2,1)} %all_refs_0_.1, bf16[256,256]{1,0:T(8,128)(2,1)} %all_refs_1_.1, bf16[64,256]{1,0:T(8,128)(2,1)} %bitcast.6, bf16[64,256]{1,0:T(8,128)(2,1)} %bitcast.7, bf16[256,256]{1,0:T(8,128)(2,1)} %all_refs_4_.1, ...), custom_call_target="tpu_custom_call" | custom-call | tf_op jit(solution)/shard_map/pallas_call | solution.py:930
  73.7 1.3 %add_convert_fusion = bf16[256,2048]{1,0:T(8,128)(2,1)} fusion(f32[256,2048]{1,0:T(8,128)S(1)} %get-tuple-element.7, bf16[256,2048]{1,0:T(8,128)(2,1)S(1)} %get-tuple-element.8), kind=kLoop, calls=%fused_computation | loop fusion | flops 1572864 | bytes 4194304 | tf_op jit(solution)/shard_map/convert_element_type | solution.py:940

commit v4 on v3

--- a/solution.py
+++ b/solution.py
@@ -243,7 +243,7 @@
     def take(self, group, step, piece=None):
         for number in range(len(self.groups[group])):
             for way in (1, -1):
-                if piece not in (None, number) or self.part(group, step, number, way) is None:
+                if piece not in (None, number * 2 // len(self.groups[group])) or self.part(group, step, number, way) is None:
                     continue
                 with jax.named_scope(f"ring{group}_{step}_{number}"):
                     self.copies[group, step, number, way].wait_recv()
@@ -327,32 +327,31 @@
     def out_columns(owner):
         return pl.ds(pl.multiple_of(owner * columns, LANES), columns)
 
-    cut = depth // 2
-
-    def value_piece(o):
-        return value_all.at[rows_of(o, 0, depth), :]
-
-    def gate_piece(o):
-        return gate_all.at[rows_of(o, 0, depth), :]
-
-    def kv_piece(low, high):
-        return lambda o: kv_all.at[pl.ds(low, high - low), kv_columns(o)]
-
-    def query_piece(low, high):
-        return lambda o: query_all.at[rows_of(o, low, high), :]
+    cut = depth // 4
+
+    def piece_of(target, low, high):
+        return lambda o: target.at[rows_of(o, low, high), :]
+
+    def split_piece(target, low, high):
+        middle = (low + high) // 2
+        return tuple(
+            piece_of(target, *span) for span in ((low, high), (low, middle), (middle, high))
+        )
 
     def proj_piece(piece):
-        return lambda o: proj_all.at[o, piece]
-
-    early, late = query_piece(0, cut), query_piece(cut, depth)
-    left_piece, right_piece = proj_piece(0), proj_piece(1)
+        spans = ((0, width + channels), (0, width), (width, width + channels))
+        return tuple(
+            (lambda o, low=low, high=high: proj_all.at[o, piece, pl.ds(low, high - low), :])
+            for low, high in spans
+        )
+
     ring = Ring(
         sp,
         (
-            ((value_piece, value_piece, None), (gate_piece, None, gate_piece)),
-            ((kv_piece(0, 2 * head), kv_piece(0, head), kv_piece(head, 2 * head)),),
-            ((early, early, None), (late, None, late)),
-            ((left_piece, left_piece, None), (right_piece, None, right_piece)),
+            (split_piece(value_all, 0, depth), split_piece(gate_all, 0, depth)),
+            (split_piece(kv_all, 0, depth),),
+            tuple(split_piece(query_all, i * cut, (i + 1) * cut) for i in range(4)),
+            (proj_piece(0), proj_piece(1)),
         ),
         sems,
     )
@@ -367,8 +366,8 @@
     local = []
     for source, target in (
             (tokens, whole.at[t]),
-            (ref.key_w, kv_all.at[pl.ds(0, head), kv_columns(s)]),
-            (ref.value_w, kv_all.at[pl.ds(head, head), kv_columns(s)]),
+            (ref.key_w, ref.kv_own.at[pl.ds(0, head), :]),
+            (ref.value_w, ref.kv_own.at[pl.ds(head, head), :]),
             (ref.mix_gain, mix_rows),
             (query_w, query_all.at[rows_of(s, 0, depth), :]),
             (ref.conv_value_w, value_all.at[rows_of(s, 0, depth), :]),
@@ -391,7 +390,8 @@
 
     ring.first(0, (ref.conv_value_w, ref.conv_gate_w))
     over = []
-    for i in range(4):
+    row_order = (0, 3, 1, 2)
+    for i in row_order:
         rows = pl.ds(i * block, block)
         over.append(push(tokens.at[rows, :], whole.at[t, rows, :], {"tp": outer}))
     beside = push(tokens, whole.at[t], {"tp": inner})
@@ -399,6 +399,8 @@
         for copy in local:
             copy.wait()
 
+    turned = jnp.transpose(ref.kv_own[...].astype(jnp.float32))
+    kv_all[rows_of(s, 0, depth), :] = turned.astype(jnp.bfloat16)
     square = (width, width)
     spread_heads[...] = jnp.where(
         row_index(square) // head == lane_index(square) // head, 1.0 / head, 0.0
@@ -412,7 +414,7 @@
     query_gain, key_gain = ref.query_gains[...], ref.key_gains[...]
     plain_lanes = jnp.ones_like(key_gain)
     head_gains[0:1, :] = jnp.concatenate([query_gain * exponent] * 4, axis=1)
-    head_gains[1:2, :] = jnp.concatenate([key_gain, plain_lanes, plain_lanes, key_gain], axis=1)
+    head_gains[1:2, :LANES] = jnp.concatenate([key_gain, plain_lanes], axis=1)
     ones_low = jnp.where(lane < head, 1.0, 0.0)
     for i in range(value_low.shape[0] // LANES):
         rows = pl.ds(i * LANES, LANES)
@@ -450,7 +452,7 @@
     def forward_tokens(i):
         with jax.named_scope("wait_over"):
             over[i].wait_recv()
-        source = whole.at[outer, pl.ds(i * block, block), :]
+        source = whole.at[outer, pl.ds(row_order[i] * block, block), :]
         forwards.append(push(source, source, {"tp": inner}))
 
     def norm_block(i):
@@ -460,7 +462,8 @@
             forwards[i].wait_recv()
         with jax.named_scope("norm"):
             per = block // step_rows
-            lax.fori_loop(i * per, (i + 1) * per, norm_rows, 0)
+            begin = row_order[i] * per
+            lax.fori_loop(begin, begin + per, norm_rows, 0)
 
     edge_out, edge_in = ref.edge_out, ref.edge_in
 
@@ -520,26 +523,44 @@
                 gated[j, start : start + half_pad, :] = values[:, j * LANES : (j + 1) * LANES]
 
     def head_scale(part):
-        mean = matmul((part * part).astype(jnp.bfloat16), spread_heads[...])
+        lanes = part.shape[1]
+        mean = matmul((part * part).astype(jnp.bfloat16), spread_heads[:lanes, :lanes])
         return lax.rsqrt(mean + EPSILON)
 
     halo_out, halo_in = ref.halo_out, ref.halo_in
 
+    def store_key_values(rows, low, inside=None):
+        high = pltpu.roll(low, head, 1)
+        is_low = lane_index(low.shape) < head
+        key_low[rows, :] = jnp.where(is_low, low, 0.0).astype(jnp.bfloat16)
+        key_high[rows, :] = jnp.where(is_low, 0.0, high).astype(jnp.bfloat16)
+        keep_low = is_low if inside is None else is_low & inside
+        keep_high = ~is_low if inside is None else ~is_low & inside
+        value_low[rows, :LANES] = jnp.where(keep_low, high, 0.0).astype(jnp.bfloat16)
+        value_high[rows, :LANES] = jnp.where(keep_high, low, 0.0).astype(jnp.bfloat16)
+
     @scoped("keys")
-    def key_value_block(i):
-        keys, vals = kv_all[:head, :], kv_all[head:, :]
-        weights = jnp.concatenate([keys, vals, vals, keys], axis=0)
-        part = contract_last(normed[i * block : (i + 1) * block, :], weights)
-        scaled = part * head_scale(part) * head_gains[1:2, :]
-        is_low = lane_index((block, LANES)) < head
-        rows = slice(WINDOW + i * block, WINDOW + (i + 1) * block)
-        key_low[rows, :] = jnp.where(is_low, scaled[:, :LANES], 0.0).astype(jnp.bfloat16)
-        value_high[rows, :LANES] = jnp.where(is_low, 0.0, part[:, :LANES]).astype(jnp.bfloat16)
-        value_low[rows, :LANES] = jnp.where(is_low, part[:, LANES:], 0.0).astype(jnp.bfloat16)
-        key_high[rows, :] = jnp.where(is_low, 0.0, scaled[:, LANES:]).astype(jnp.bfloat16)
-        if i in (0, 3):
-            low = jnp.where(is_low, scaled[:, :LANES], part[:, :LANES]).astype(jnp.bfloat16)
-            halo_out[i // 3] = low[:WINDOW] if i == 0 else low[block - WINDOW :]
+    def key_value_block(i, edge=None):
+        begin = aligned(i * block, block)
+        part = matmul(normed[pl.ds(begin, block), :], kv_all[...])
+        scaled = part * head_scale(part) * head_gains[1:2, :LANES]
+        low = jnp.where(lane_index(part.shape) < head, scaled, part)
+        store_key_values(pl.ds(aligned(begin + WINDOW, WINDOW), block), low)
+        if edge is not None:
+            halo_out[edge] = low.astype(jnp.bfloat16)
+
+    def push_halo(edge, last):
+        where = {"sp": (s + sp + 2 * last - 1) % sp}
+        source = halo_out.at[edge, pl.ds(aligned(last * (block - WINDOW), WINDOW), WINDOW), :]
+        return push(source, halo_in.at[1 - last], where)
+
+    def fill_halo(copy, last):
+        with jax.named_scope("wait_halo"):
+            copy.wait_recv()
+        outside = (s == 0) & (last == 1) | (s == sp - 1) & (last == 0)
+        start = aligned((1 - last) * (WINDOW + count), WINDOW)
+        low = halo_in[1 - last].astype(jnp.float32)
+        store_key_values(pl.ds(start, WINDOW), low, ~outside)
 
     ring.take(0, 1)
     forward_tokens(0)
@@ -556,44 +577,42 @@
     norm_block(2)
     ring.take(0, half)
     gate_block(0)
-    gate_block(1)
-    ring.take(1, 2)
-    forward_tokens(3)
-    gate_block(2)
-    ring.take(2, 1, 0)
-    norm_block(3)
-    ring.take(2, 1, 1)
     gate_block(3)
     edges = [
         push(edge_out.at[1], edge_in.at[0], {"sp": following}),
         push(edge_out.at[0], edge_in.at[1], {"sp": preceding}),
     ]
-    convolve(quarter, quarter + 1)
+    ring.take(1, 2)
+    forward_tokens(3)
+    gate_block(1)
+    ring.take(2, 1, 0)
+    norm_block(3)
+    ring.take(2, 1, 1)
+    gate_block(2)
+    convolve(1, quarter + 1)
     for step in range(3, half):
         ring.take(1, step)
-    convolve(quarter + 1, 3 * quarter - 1)
+    convolve(quarter + 1, 2 * quarter + 1)
     ring.take(2, 2, 0)
-    convolve(3 * quarter - 1, 3 * quarter)
-    convolve(1, quarter)
+    convolve(2 * quarter + 1, blocks - 1)
     ring.take(2, 2, 1)
-    convolve(3 * quarter, blocks - 1)
-    ring.take(1, half)
     fill_edges()
     convolve(0, 1)
-    for step in range(3, half - 1):
-        ring.take(2, step)
+    ring.take(1, half)
     convolve(blocks - 1, blocks)
     stat_pair, part_pair = next(sems), next(sems)
     for i, peer in enumerate((inner, outer, cross)):
         push(stat_out, stat_in.at[i], {"tp": peer}, stat_pair)
+    for step in range(3, half - 1):
+        ring.take(2, step)
     ring.take(2, half - 1, 0)
-    key_value_block(0)
-    right_halo = push(halo_out.at[0], halo_in.at[1], {"sp": preceding})
+    key_value_block(3 * a, 0)
+    far_halo = push_halo(0, a)
     ring.take(2, half - 1, 1)
-    key_value_block(3)
-    halos = [push(halo_out.at[1], halo_in.at[0], {"sp": following}), right_halo]
+    key_value_block(3 * (1 - a), 1)
+    ring.first(3)
+    near_halo = push_halo(1, 1 - a)
     key_value_block(1)
-    ring.first(3)
     key_value_block(2)
 
     def feature_rows(i, carry):
@@ -619,22 +638,24 @@
         return push(mixers.at[give[f], width:], mixers_other.at[f, :, width:], {"tp": inner})
 
     @scoped("partial")
-    def partial_block(i, rows):
+    def partial_block(f, i):
+        rows = pl.ds(pl.multiple_of((starts[f] + i) * block, block), block)
         owners = [ring.owner(slot) for slot in range(sp - 1)]
         left = jnp.concatenate([normed[rows, kv_columns(o)] for o in owners], axis=1)
         right = jnp.concatenate([query_all[rows_of(o, 0, depth), :] for o in owners], axis=0)
-        query_part[i] = matmul(left, right)
+        query_part[i * block : (i + 1) * block, :] = matmul(left, right)
+
+    both = [pl.ds(pl.multiple_of(base * block, block), 2 * block) for base in starts]
 
     @scoped("queries")
-    def query_block(i, rows):
+    def query_rows(f):
         owner = ring.owner(sp - 1)
-        last = matmul(normed[rows, kv_columns(owner)], query_all[rows_of(owner, 0, depth), :])
-        part = query_part[i] + last
-        queries[rows, :] = (part * head_scale(part) * head_gains[0:1, :]).astype(jnp.bfloat16)
-
-    far_rows = [give[0], keep[0]]
-    for i, rows in enumerate(far_rows):
-        partial_block(i, rows)
+        last = matmul(normed[both[f], kv_columns(owner)], query_all[rows_of(owner, 0, depth), :])
+        part = query_part[...] + last
+        queries[both[f], :] = (part * head_scale(part) * head_gains[0:1, :]).astype(jnp.bfloat16)
+
+    for i in range(2):
+        partial_block(0, i)
     with jax.named_scope("wait_stat"):
         remote(stat_in, stat_in, stat_pair, {"tp": inner}).wait_recv()
     every = [stat_out[...]] + [stat_in[i] for i in range(3)]
@@ -646,8 +667,7 @@
 
     given_features = [features_of(0)]
     ring.take(2, half)
-    for i, rows in enumerate(far_rows):
-        query_block(i, rows)
+    query_rows(0)
 
     shared = {}
 
@@ -656,24 +676,13 @@
         source, target = proj_all.at[owner, piece], proj_other.at[owner, piece]
         shared[slot, piece] = push(source, target, {"tp": inner})
 
-    ring.arrived = lambda group, step, piece, way: share(ring.slot(step, way), piece)
+    def arrived(group, step, piece, way):
+        if step < half or way == -1:
+            share(ring.slot(step, way), piece)
+
+    ring.arrived = arrived
     share(0, 0)
     share(0, 1)
-    def fill_halos():
-        for side, halo in enumerate(halos):
-            with jax.named_scope("wait_halo"):
-                halo.wait_recv()
-            inside = s > 0 if side == 0 else s < sp - 1
-            low = halo_in[side].astype(jnp.float32)
-            high = pltpu.roll(low, head, 1)
-            is_low = lane_index(low.shape) < head
-            start = 0 if side == 0 else WINDOW + count
-            rows = slice(start, start + WINDOW)
-            key_low[rows, :] = jnp.where(is_low, low, 0.0).astype(jnp.bfloat16)
-            key_high[rows, :] = jnp.where(is_low, 0.0, high).astype(jnp.bfloat16)
-            value_low[rows, :LANES] = jnp.where(is_low & inside, high, 0.0).astype(jnp.bfloat16)
-            value_high[rows, :LANES] = jnp.where(is_low | ~inside, 0.0, low).astype(jnp.bfloat16)
-
     head_lanes = lane_index((1, LANES)) < head
     sink_rows = [
         jnp.exp(jnp.where(head_lanes, sinks[2 * i], sinks[2 * i + 1])) for i in range(2)
@@ -681,27 +690,36 @@
 
     @scoped("attend")
     def attend_rows(first, windows):
-        for i in range(windows):
-            start = pl.multiple_of(first + i * WINDOW, WINDOW)
-            rows = pl.ds(start, WINDOW)
-            left = jnp.concatenate([queries[rows, :LANES], queries[rows, LANES:]], axis=0)
-            shares, vals = [], []
-            for j in range(3):
-                span = pl.ds(pl.multiple_of(start + j * WINDOW, WINDOW), WINDOW)
-                right = jnp.concatenate([key_low[span, :], key_high[span, :]], axis=0)
-                weight = jnp.exp2(contract_last(left, right))
-                if j != 1:
-                    mask = band[j // 2]
+        starts_at = [pl.multiple_of(first + w * WINDOW, WINDOW) for w in range(windows)]
+        lefts = [
+            jnp.concatenate([queries[pl.ds(b, WINDOW), lanes] for lanes in halves], axis=0)
+            for b in starts_at
+        ]
+        shares, vals = [[] for _ in range(windows)], []
+        for j in range(windows + 2):
+            span = pl.ds(pl.multiple_of(first + j * WINDOW, WINDOW), WINDOW)
+            readers = [w for w in range(windows) if 0 <= j - w <= 2]
+            left = jnp.concatenate([lefts[w] for w in readers], axis=0)
+            right = jnp.concatenate([key_low[span, :], key_high[span, :]], axis=0)
+            weights = jnp.exp2(contract_last(left, right))
+            for n, w in enumerate(readers):
+                weight = weights[n * 2 * WINDOW : (n + 1) * 2 * WINDOW]
+                if j - w != 1:
+                    mask = band[(j - w) // 2]
                     mask = jnp.concatenate([mask, mask], axis=0)
                     weight = weight * jnp.concatenate([mask, mask], axis=1)
-                shares.append(weight.astype(jnp.bfloat16))
-                vals += [value_low[span, :], value_high[span, :]]
-            total = matmul(jnp.concatenate(shares, axis=1), jnp.concatenate(vals, axis=0))
+                shares[w].append(weight.astype(jnp.bfloat16))
+            vals.append(jnp.concatenate([value_low[span, :], value_high[span, :]], axis=0))
+        for w, b in enumerate(starts_at):
+            right = jnp.concatenate(vals[w : w + 3], axis=0)
+            total = matmul(jnp.concatenate(shares[w], axis=1), right)
             for j in range(2):
                 piece = total[j * WINDOW : (j + 1) * WINDOW]
-                mixers[rows, j * LANES : (j + 1) * LANES] = (
+                mixers[pl.ds(b, WINDOW), halves[j]] = (
                     piece[:, :LANES] / (piece[:, LANES:] + sink_rows[j])
                 ).astype(jnp.bfloat16)
+
+    halves = (slice(0, LANES), slice(LANES, 2 * LANES))
 
     def attend_given(f, low=0, size=block):
         here = pl.multiple_of((starts[f] + 1 - c) * block + low, WINDOW)
@@ -729,17 +747,9 @@
         with jax.named_scope("wait_shared"):
             shared[slot, piece].wait_recv()
 
-    def send_rows(slot, low, size):
-        rows = pl.ds(aligned(low, WINDOW), size)
-        result = project(0, slot, (0, 1), low, size).astype(jnp.bfloat16)
-        for piece in range(2):
-            far_out[slot, piece, rows, :] = result[:, piece * thin : (piece + 1) * thin]
-        for piece in range(2):
-            target = far_in.at[rows, half_columns(slot, piece)]
-            push(far_out.at[slot, piece, rows, :], target, {"tp": outer}, part_pair)
-
     def send_piece(slot, piece):
-        wait_shared(slot, piece)
+        if slot:
+            wait_shared(slot, piece)
         far_out[slot, piece] = project(0, slot, (piece,)).astype(jnp.bfloat16)
         target = far_in.at[:, half_columns(slot, piece)]
         push(far_out.at[slot, piece], target, {"tp": outer}, part_pair)
@@ -751,38 +761,32 @@
     def keep_part(slot):
         near_out[:, out_columns(ring.owner(slot))] = project(1, slot)
 
-    split = block // 2
-    order = (a * split, (1 - a) * split)
-    given_heads = [attend_given(0, order[0], split)]
-    attend_kept(0, order[0], split)
+    fill_halo(far_halo, a)
+    given_heads = [attend_given(0)]
+    attend_kept(0)
     given_features[0].wait_recv()
     for piece in range(2):
         wait_shared(0, piece)
     with jax.named_scope("wait_given"):
         given_heads[0].wait_recv()
-    send_rows(0, order[0], split)
-    fill_halos()
-    given_heads.append(attend_given(0, order[1], split))
-    attend_kept(0, order[1], split)
-    with jax.named_scope("wait_given"):
-        given_heads[1].wait_recv()
-    send_rows(0, order[1], split)
+    for piece in range(2):
+        send_piece(0, piece)
 
     def near_heads():
+        fill_halo(near_halo, 1 - a)
         given_heads.append(attend_given(1))
 
     def near_kept():
         attend_kept(1)
         with jax.named_scope("wait_given"):
             given_features[1].wait_recv()
-            given_heads[2].wait_recv()
+            given_heads[1].wait_recv()
 
     work = [
-        lambda: partial_block(0, give[1]),
-        lambda: query_block(0, give[1]),
+        lambda: partial_block(1, 0),
+        lambda: partial_block(1, 1),
+        lambda: query_rows(1),
         lambda: given_features.append(features_of(1)),
-        lambda: partial_block(1, keep[1]),
-        lambda: query_block(1, keep[1]),
         near_heads,
         near_kept,
         lambda: keep_part(0),
@@ -792,7 +796,7 @@
         for _ in range(min(most, len(work))):
             work.pop(0)()
 
-    counts = {(1, 0): (1, 0), (1, 1): (1, 3), (2, 0): (1, 1), (2, 1): (1, 2)}
+    counts = {(1, 0): (1, 0), (1, 1): (1, 2), (2, 0): (1, 1), (2, 1): (1, 2)}
     for step in range(1, half + 1):
         slots = (2 * step - 1, 2 * step) if step < half else (2 * step - 1,)
         for piece in range(2):
@@ -815,8 +819,7 @@
 
 
 def recv_count(sp):
-    pieces = 7 * 2 * (sp // 2 - 1) + 4 * 2
-    return pieces + 2 * sp + 9 + 2 + 2 + 2 + 2 + 3
+    return 9 * 2 * (sp // 2) + 2 * sp + 9 + 2 + 2 + 1 + 1 + 2 + 2
 
 
 def fits(sp, tp, tokens, query_weight, key_weight, conv_weight, attn_proj, taps, head):
@@ -890,7 +893,8 @@
         whole=vmem((4, count, features), bf16),
         normed=vmem((count, model), bf16),
         query_all=vmem((model, width), bf16),
-        kv_all=vmem((2 * head, model), bf16),
+        kv_own=vmem((2 * head, depth), bf16),
+        kv_all=vmem((model, 2 * head), bf16),
         value_all=vmem((model, channels), bf16),
         gate_all=vmem((model, channels), bf16),
         proj_all=vmem((sp, 2, width + channels, columns // 2), bf16),
@@ -913,12 +917,12 @@
         stat_in=vmem((3, stat, LANES), f32),
         stat_rows=vmem((stat, LANES), f32),
         queries=vmem((count, width), bf16),
-        query_part=vmem((2, block, width), f32),
+        query_part=vmem((2 * block, width), f32),
         key_low=vmem((padded_rows, LANES), bf16),
         key_high=vmem((padded_rows, LANES), bf16),
         value_low=vmem((padded_rows, 2 * LANES), bf16),
         value_high=vmem((padded_rows, 2 * LANES), bf16),
-        halo_out=vmem((2, WINDOW, LANES), bf16),
+        halo_out=vmem((2, block, LANES), bf16),
         halo_in=vmem((2, WINDOW, LANES), bf16),
         mixers=vmem((count, width + channels), bf16),
         mixers_other=vmem((2, block, width + channels), bf16),

time: 75.1 us -> 74.3 us (0.989)
  Pallas kernels: 73.7 us -> 72.8 us
    pallas_call x1, Pallas kernels: 73.7 us -> 72.8 us  [fused(): pl.pallas_call(functools.partial(fused_kernel, sp, (*inputs, *outputs, *s...]
where the time goes in v4:
time: 74.3 us; the launch traced here: 74.1 us
  Pallas kernels  72.8 us (98%)
  other arithmetic  1.26 us (2%)
    pallas_call x1, Pallas kernels, fused(): pl.pallas_call(functools.partial(fused_kernel, sp, (*inputs, *outputs, *s...  72.8 us

profile of v4, /device:TPU:0, one launch (start us, length us, event | category | flops | bytes accessed | tf_op | source)
XLA Modules:
  0.0 74.1 jit_solution(11771291903027060489)
XLA Ops:
  0.0 72.8 %shard_map.136 = (f32[256,2048]{1,0:T(8,128)S(1)}, bf16[256,2048]{1,0:T(8,128)(2,1)S(1)}) custom-call(bf16[1024,512]{1,0:T(8,128)(2,1)} %all_refs_0_.1, bf16[256,256]{1,0:T(8,128)(2,1)} %all_refs_1_.1, bf16[64,256]{1,0:T(8,128)(2,1)} %bitcast.6, bf16[64,256]{1,0:T(8,128)(2,1)} %bitcast.7, bf16[256,256]{1,0:T(8,128)(2,1)} %all_refs_4_.1, ...), custom_call_target="tpu_custom_call" | custom-call | tf_op jit(solution)/shard_map/pallas_call | solution.py:934
  72.9 1.3 %add_convert_fusion = bf16[256,2048]{1,0:T(8,128)(2,1)} fusion(f32[256,2048]{1,0:T(8,128)S(1)} %get-tuple-element.7, bf16[256,2048]{1,0:T(8,128)(2,1)S(1)} %get-tuple-element.8), kind=kLoop, calls=%fused_computation | loop fusion | flops 1572864 | bytes 4194304 | tf_op jit(solution)/shard_map/convert_element_type | solution.py:944

commit v5 on v4

--- a/solution.py
+++ b/solution.py
@@ -229,16 +229,23 @@
             return whole
         return None if step > self.half else up if way == 1 else down
 
-    def send(self, group, step, piece, way, source=None):
+    def send(self, group, step, piece, way, source=None, hold=False):
         ref = self.part(group, step, piece, way)(self.at(-way * (step - 1)))
         copy = remote(ref if source is None else source, ref, next(self.sems), {"sp": self.at(way)})
-        copy.start()
         self.copies[group, step, piece, way] = copy
-
-    def first(self, group, sources=None):
+        if not hold:
+            copy.start()
+
+    def first(self, group, sources=None, hold=False):
         for piece in range(len(self.groups[group])):
             for way in (1, -1):
-                self.send(group, 1, piece, way, None if sources is None else sources[piece])
+                source = None if sources is None else sources[piece]
+                self.send(group, 1, piece, way, source, hold)
+
+    def start_first(self, group):
+        for piece in range(len(self.groups[group])):
+            for way in (1, -1):
+                self.copies[group, 1, piece, way].start()
 
     def take(self, group, step, piece=None):
         for number in range(len(self.groups[group])):
@@ -303,7 +310,8 @@
     a, c = t // 2, t % 2
     inner, outer = t + 1 - 2 * c, (t + 2) % 4
     cross = outer + 1 - 2 * c
-    send_sem, recv_sem, local_sem = ref.send_sem, ref.recv_sem, ref.local_sem
+    send_sem, recv_sem = ref.send_sem, ref.recv_sem
+    local_sem, ahead_sem = ref.local_sem, ref.ahead_sem
 
     def sem_pairs():
         for i in range(recv_sem.shape[0]):
@@ -363,6 +371,14 @@
     near_devices += [{"tp": inner}, {"tp": outer}, {"tp": cross}]
     for where in near_devices:
         pl.semaphore_signal(barrier, inc=1, device_id=where, device_id_type=MESH)
+    ahead = []
+    for source, target in (
+        (ref.conv_value_w, value_all.at[rows_of(s, 0, depth), :]),
+        (ref.conv_gate_w, gate_all.at[rows_of(s, 0, depth), :]),
+    ):
+        copy = pltpu.make_async_copy(source, target, ahead_sem)
+        copy.start()
+        ahead.append(copy)
     local = []
     for source, target in (
             (tokens, whole.at[t]),
@@ -370,8 +386,6 @@
             (ref.value_w, ref.kv_own.at[pl.ds(head, head), :]),
             (ref.mix_gain, mix_rows),
             (query_w, query_all.at[rows_of(s, 0, depth), :]),
-            (ref.conv_value_w, value_all.at[rows_of(s, 0, depth), :]),
-            (ref.conv_gate_w, gate_all.at[rows_of(s, 0, depth), :]),
             (ref.attn_p.at[:, :thin], proj_all.at[s, 0, pl.ds(0, width), :]),
             (ref.attn_p.at[:, thin:], proj_all.at[s, 1, pl.ds(0, width), :]),
             (ref.conv_p.at[:, :thin], proj_all.at[s, 0, pl.ds(width, channels), :]),
@@ -388,7 +402,10 @@
     with jax.named_scope("wait_barrier"):
         pl.semaphore_wait(barrier, len(near_devices))
 
-    ring.first(0, (ref.conv_value_w, ref.conv_gate_w))
+    with jax.named_scope("wait_ahead"):
+        for copy in ahead:
+            copy.wait()
+    ring.first(0)
     over = []
     row_order = (0, 3, 1, 2)
     for i in row_order:
@@ -589,13 +606,14 @@
     norm_block(3)
     ring.take(2, 1, 1)
     gate_block(2)
-    convolve(1, quarter + 1)
+    convolve(1, 2)
     for step in range(3, half):
         ring.take(1, step)
-    convolve(quarter + 1, 2 * quarter + 1)
+    convolve(2, quarter + 2)
     ring.take(2, 2, 0)
-    convolve(2 * quarter + 1, blocks - 1)
+    convolve(quarter + 2, 2 * quarter + 2)
     ring.take(2, 2, 1)
+    convolve(2 * quarter + 2, blocks - 1)
     fill_edges()
     convolve(0, 1)
     ring.take(1, half)
@@ -603,17 +621,19 @@
     stat_pair, part_pair = next(sems), next(sems)
     for i, peer in enumerate((inner, outer, cross)):
         push(stat_out, stat_in.at[i], {"tp": peer}, stat_pair)
+    key_value_block(3 * a, 0)
+    far_halo = push_halo(0, a)
     for step in range(3, half - 1):
         ring.take(2, step)
     ring.take(2, half - 1, 0)
-    key_value_block(3 * a, 0)
-    far_halo = push_halo(0, a)
+    key_value_block(3 * (1 - a), 1)
     ring.take(2, half - 1, 1)
-    key_value_block(3 * (1 - a), 1)
-    ring.first(3)
+    ring.first(3, hold=True)
+    pl.when(c == 0)(lambda: ring.start_first(3))
     near_halo = push_halo(1, 1 - a)
     key_value_block(1)
     key_value_block(2)
+    pl.when(c == 1)(lambda: ring.start_first(3))
 
     def feature_rows(i, carry):
         rows = pl.ds(pl.multiple_of(i * LANES, LANES), LANES)
@@ -928,6 +948,7 @@
         mixers_other=vmem((2, block, width + channels), bf16),
         far_out=vmem((sp, 2, block, columns // 2), bf16),
         local_sem=dma,
+        ahead_sem=dma,
         send_sem=dma,
         recv_sem=dma((recv_count(sp),)),
     )

time: 74.3 us -> 74 us (level)
  no operation moved by 1% of the time
where the time goes in v5:
time: 74 us; the launch traced here: 73.9 us
  Pallas kernels  72.6 us (98%)
  other arithmetic  1.26 us (2%)
    pallas_call x1, Pallas kernels, fused(): pl.pallas_call(functools.partial(fused_kernel, sp, (*inputs, *outputs, *s...  72.6 us

profile of v5, /device:TPU:0, one launch (start us, length us, event | category | flops | bytes accessed | tf_op | source)
XLA Modules:
  0.0 73.9 jit_solution(11886895132445282897)
XLA Ops:
  0.0 72.6 %shard_map.136 = (f32[256,2048]{1,0:T(8,128)S(1)}, bf16[256,2048]{1,0:T(8,128)(2,1)S(1)}) custom-call(bf16[1024,512]{1,0:T(8,128)(2,1)} %all_refs_0_.1, bf16[256,256]{1,0:T(8,128)(2,1)} %all_refs_1_.1, bf16[64,256]{1,0:T(8,128)(2,1)} %bitcast.6, bf16[64,256]{1,0:T(8,128)(2,1)} %bitcast.7, bf16[256,256]{1,0:T(8,128)(2,1)} %all_refs_4_.1, ...), custom_call_target="tpu_custom_call" | custom-call | tf_op jit(solution)/shard_map/pallas_call | solution.py:955
  72.6 1.3 %add_convert_fusion = bf16[256,2048]{1,0:T(8,128)(2,1)} fusion(f32[256,2048]{1,0:T(8,128)S(1)} %get-tuple-element.7, bf16[256,2048]{1,0:T(8,128)(2,1)S(1)} %get-tuple-element.8), kind=kLoop, calls=%fused_computation | loop fusion | flops 1572864 | bytes 4194304 | tf_op jit(solution)/shard_map/convert_element_type | solution.py:965

commit v6 on v5

--- a/solution.py
+++ b/solution.py
@@ -213,13 +213,15 @@
 
 
 class Ring:
-    def __init__(self, size, groups, sems):
+    def __init__(self, size, groups, sems, reuse):
         place_of, index_of = snake(size)
         place = place_of(lax.axis_index("sp"))
         self.at = lambda shift: index_of((place + shift + size) % size)
         self.half = size // 2
         self.groups = groups
         self.sems = sems
+        self.reuse = reuse
+        self.pairs = {}
         self.copies = {}
         self.arrived = None
 
@@ -231,7 +233,10 @@
 
     def send(self, group, step, piece, way, source=None, hold=False):
         ref = self.part(group, step, piece, way)(self.at(-way * (step - 1)))
-        copy = remote(ref if source is None else source, ref, next(self.sems), {"sp": self.at(way)})
+        key = self.reuse.get((group, piece), (group, piece)) + (step, way)
+        if key not in self.pairs:
+            self.pairs[key] = next(self.sems)
+        copy = remote(ref if source is None else source, ref, self.pairs[key], {"sp": self.at(way)})
         self.copies[group, step, piece, way] = copy
         if not hold:
             copy.start()
@@ -362,6 +367,7 @@
             (proj_piece(0), proj_piece(1)),
         ),
         sems,
+        {(2, 0): (0, 0), (2, 1): (0, 1), (3, 0): (2, 2), (3, 1): (2, 3)},
     )
     half = ring.half
 
@@ -839,7 +845,7 @@
 
 
 def recv_count(sp):
-    return 9 * 2 * (sp // 2) + 2 * sp + 9 + 2 + 2 + 1 + 1 + 2 + 2
+    return 5 * 2 * (sp // 2) + 2 * sp + 9 + 2 + 2 + 1 + 1 + 2 + 2
 
 
 def fits(sp, tp, tokens, query_weight, key_weight, conv_weight, attn_proj, taps, head):

time: 74 us -> 73.7 us (level)
  no operation moved by 1% of the time
where the time goes in v6:
time: 73.7 us; the launch traced here: 73.6 us
  Pallas kernels  72.3 us (98%)
  other arithmetic  1.26 us (2%)
    pallas_call x1, Pallas kernels, fused(): pl.pallas_call(functools.partial(fused_kernel, sp, (*inputs, *outputs, *s...  72.3 us

profile of v6, /device:TPU:0, one launch (start us, length us, event | category | flops | bytes accessed | tf_op | source)
XLA Modules:
  0.0 73.6 jit_solution(10352172624638556646)
XLA Ops:
  0.0 72.3 %shard_map.136 = (f32[256,2048]{1,0:T(8,128)S(1)}, bf16[256,2048]{1,0:T(8,128)(2,1)S(1)}) custom-call(bf16[1024,512]{1,0:T(8,128)(2,1)} %all_refs_0_.1, bf16[256,256]{1,0:T(8,128)(2,1)} %all_refs_1_.1, bf16[64,256]{1,0:T(8,128)(2,1)} %bitcast.6, bf16[64,256]{1,0:T(8,128)(2,1)} %bitcast.7, bf16[256,256]{1,0:T(8,128)(2,1)} %all_refs_4_.1, ...), custom_call_target="tpu_custom_call" | custom-call | tf_op jit(solution)/shard_map/pallas_call | solution.py:961
  72.3 1.3 %add_convert_fusion = bf16[256,2048]{1,0:T(8,128)(2,1)} fusion(f32[256,2048]{1,0:T(8,128)S(1)} %get-tuple-element.7, bf16[256,2048]{1,0:T(8,128)(2,1)S(1)} %get-tuple-element.8), kind=kLoop, calls=%fused_computation | loop fusion | flops 1572864 | bytes 4194304 | tf_op jit(solution)/shard_map/convert_element_type | solution.py:971

commit v7 on v6

--- a/solution.py
+++ b/solution.py
@@ -412,11 +412,11 @@
         for copy in ahead:
             copy.wait()
     ring.first(0)
-    over = []
+    over, token_pairs = [], [next(sems) for _ in range(8)]
     row_order = (0, 3, 1, 2)
     for i in row_order:
         rows = pl.ds(i * block, block)
-        over.append(push(tokens.at[rows, :], whole.at[t, rows, :], {"tp": outer}))
+        over.append(push(tokens.at[rows, :], whole.at[t, rows, :], {"tp": outer}, token_pairs[len(over)]))
     beside = push(tokens, whole.at[t], {"tp": inner})
     with jax.named_scope("wait_local"):
         for copy in local:
@@ -476,7 +476,7 @@
         with jax.named_scope("wait_over"):
             over[i].wait_recv()
         source = whole.at[outer, pl.ds(row_order[i] * block, block), :]
-        forwards.append(push(source, source, {"tp": inner}))
+        forwards.append(push(source, source, {"tp": inner}, token_pairs[4 + i]))
 
     def norm_block(i):
         with jax.named_scope("wait_forward"):
@@ -696,11 +696,12 @@
     query_rows(0)
 
     shared = {}
+    spare = iter([pair for key, pair in ring.pairs.items() if key[0] == 1] + token_pairs)
 
     def share(slot, piece):
         owner = ring.owner(slot)
         source, target = proj_all.at[owner, piece], proj_other.at[owner, piece]
-        shared[slot, piece] = push(source, target, {"tp": inner})
+        shared[slot, piece] = push(source, target, {"tp": inner}, next(spare, None))
 
     def arrived(group, step, piece, way):
         if step < half or way == -1:
@@ -845,7 +846,7 @@
 
 
 def recv_count(sp):
-    return 5 * 2 * (sp // 2) + 2 * sp + 9 + 2 + 2 + 1 + 1 + 2 + 2
+    return 5 * 2 * (sp // 2) + max(0, 2 * sp - sp - 8) + 9 + 2 + 2 + 1 + 1 + 2 + 2
 
 
 def fits(sp, tp, tokens, query_weight, key_weight, conv_weight, attn_proj, taps, head):

time: 73.7 us -> 73.6 us (level)
  no operation moved by 1% of the time
where the time goes in v7:
time: 73.6 us; the launch traced here: 73.5 us
  Pallas kernels  72.2 us (98%)
  other arithmetic  1.26 us (2%)
    pallas_call x1, Pallas kernels, fused(): pl.pallas_call(functools.partial(fused_kernel, sp, (*inputs, *outputs, *s...  72.2 us

profile of v7, /device:TPU:0, one launch (start us, length us, event | category | flops | bytes accessed | tf_op | source)
XLA Modules:
  0.0 73.5 jit_solution(16922096278646499563)
XLA Ops:
  0.0 72.2 %shard_map.136 = (f32[256,2048]{1,0:T(8,128)S(1)}, bf16[256,2048]{1,0:T(8,128)(2,1)S(1)}) custom-call(bf16[1024,512]{1,0:T(8,128)(2,1)} %all_refs_0_.1, bf16[256,256]{1,0:T(8,128)(2,1)} %all_refs_1_.1, bf16[64,256]{1,0:T(8,128)(2,1)} %bitcast.6, bf16[64,256]{1,0:T(8,128)(2,1)} %bitcast.7, bf16[256,256]{1,0:T(8,128)(2,1)} %all_refs_4_.1, ...), custom_call_target="tpu_custom_call" | custom-call | tf_op jit(solution)/shard_map/pallas_call | solution.py:962
  72.2 1.3 %add_convert_fusion = bf16[256,2048]{1,0:T(8,128)(2,1)} fusion(f32[256,2048]{1,0:T(8,128)S(1)} %get-tuple-element.7, bf16[256,2048]{1,0:T(8,128)(2,1)S(1)} %get-tuple-element.8), kind=kLoop, calls=%fused_computation | loop fusion | flops 1572864 | bytes 4194304 | tf_op jit(solution)/shard_map/convert_element_type | solution.py:972
